TPU v7x, 32 devices: a whole 2x2x4 slice. The times are simulated.
32 devices in a mesh: sp: 16 (over z, y, x), tp: 2 (over core).
Axes of the slice: x: 2, y: 2, z: 4, core: 2. Of those that a mesh axis runs over, the one named last changes fastest.
Arguments:
- wide_inputs: bfloat16 [2048, 512], P('sp', 'tp'), may hold values from -6 to 6
- narrow_inputs: bfloat16 [2048, 512], P('sp', 'tp'), may hold values from -6 to 6
- wide_poles: float32 [2, 2, 32, 64], P(None, None, 'tp'), may hold values from -3.1416 to 3.1416, as said below
- narrow_poles: float32 [2, 2, 32, 32], P(None, None, 'tp'), may hold values from -3.1416 to 3.1416, as said below
- step_sizes: float32 [2, 2, 32], P(None, None, 'tp'), may hold values from 0 to 1, as said below
- forget: float32 [2, 2, 32, 2048], P(None, None, 'tp', 'sp'), may hold values from 0 to 2.2
- wide_in_map: float32 [2, 2, 32, 16, 64], P(None, None, 'tp'), may hold values from -2.5 to 2.5
- narrow_in_map: float32 [2, 2, 32, 16, 32], P(None, None, 'tp'), may hold values from -2.5 to 2.5
- wide_out_map: float32 [2, 2, 32, 16, 64], P(None, None, 'tp'), may hold values from -1.25 to 1.25
- narrow_out_map: float32 [2, 2, 32, 16, 32], P(None, None, 'tp'), may hold values from -2 to 2
- skip_weight: bfloat16 [2, 512], P(None, 'tp'), may hold values from -6 to 6
- gate_mix: bfloat16 [2, 32, 16, 16], P(None, 'tp'), may hold values from -1.5 to 1.5
- residual: bfloat16 [2048, 2048], P(('sp', 'tp')), may hold values from -6 to 6
- mixer_gain: float32 [1024], replicated, may hold values from 0.1 to 1.9
- out_proj: bfloat16 [1024, 2048], replicated, may hold values from -0.1875 to 0.1875
- ffn_gain: float32 [2048], replicated, may hold values from 0.1 to 1.9
- routes: int32 [2048, 2], P(('sp', 'tp')), may hold values from 0 to 31, all different within a row; in each aligned block of 64 rows (0 to 63, 64 to 127, ...) at most 8 rows name the same one
- route_weights: float32 [2048, 2], P(('sp', 'tp')), may hold values from 0.1 to 1
- gate_proj: bfloat16 [32, 2048, 1408], P(('sp', 'tp')), may hold values from -0.125 to 0.125
- up_proj: bfloat16 [32, 2048, 1408], P(('sp', 'tp')), may hold values from -0.125 to 0.125
- down_proj: bfloat16 [32, 1408, 2048], P(('sp', 'tp')), may hold values from -0.15625 to 0.15625
Outputs:
- layer_out: bfloat16 [2048, 2048], P(('sp', 'tp'))
Inputs may be any that keep to these rules, and one draw needn't show every extreme that they name: `routes`: in each aligned block of 64 rows (the rows of one device), no expert is named by more than 8 entries, and the 2 experts of a row differ. `wide_poles`: along dimension 1, entry 0 (the real part) is negative and entry 1 (the imaginary part) is at least 0.1 in magnitude. `narrow_poles`: along dimension 1, entry 0 (the real part) is negative and entry 1 (the imaginary part) is at least 0.1 in magnitude. `step_sizes`: Positive.
All inputs are finite; a program needn't handle non-finite values.
Results may differ from a plain program's by a relative error of at most 0.014.
Values may be sent and summed in bfloat16 or wider, within the bound.
A program may use at most 192 MiB of HBM per device.

v0:
```python
import functools

import jax
import jax.numpy as jnp
from jax import lax
from jax.experimental import pallas as pl
from jax.experimental.pallas import tpu as pltpu
from jax.sharding import PartitionSpec as P

epsilon = 1e-06
SUBLANES = 8
LANES = 128


def complex_power(re, im, exponent):
    out_re, out_im = None, None
    while exponent:
        if exponent & 1:
            if out_re is None:
                out_re, out_im = re, im
            else:
                out_re, out_im = out_re * re - out_im * im, out_re * im + out_im * re
        re, im = re * re - im * im, 2.0 * re * im
        exponent >>= 1
    return out_re, out_im


def packs_of(channels, groups, wide_state, narrow_state):
    per = LANES // channels
    packs, column = [], 0
    for which, states in enumerate((wide_state, narrow_state)):
        for pack in range(groups // per):
            group = which * groups + pack * per
            packs.append((group * channels, column, group, per * states, states))
            column += per * states
    return packs


def spread(rows, channels, states):
    tiled = jnp.concatenate([rows] * (LANES // channels), axis=0)
    row = lax.broadcasted_iota(jnp.int32, tiled.shape, 0) // channels
    column = lax.broadcasted_iota(jnp.int32, tiled.shape, 1) // states
    return jnp.where(row == column, tiled, 0.0).astype(jnp.bfloat16)


def fill_pack(pack, direction, channels, u_ref, in_ref, keep_ref, push_re, push_im, keep):
    channel, column, group, width, states = pack
    signal = u_ref[:, channel : channel + LANES]
    for part, target in enumerate((push_re, push_im)):
        rows = in_ref[direction, part, :, column : column + width]
        target[:, :width] = jnp.dot(
            signal, spread(rows, channels, states), preferred_element_type=jnp.float32
        )
    groups = keep_ref.shape[2]
    row = lax.broadcasted_iota(jnp.int32, (groups, width), 0)
    owner = group + lax.broadcasted_iota(jnp.int32, (groups, width), 1) // states
    keep[:, :width] = jnp.dot(
        keep_ref[direction],
        jnp.where(row == owner, 1.0, 0.0),
        precision=lax.Precision.HIGHEST,
        preferred_element_type=jnp.float32,
    )


def order(count, direction):
    return range(count) if direction == 0 else range(count - 1, -1, -1)


def ends_kernel(packs, channels, u_ref, in_ref, rate_ref, keep_ref, ends_ref, sub_ref, push_re, push_im, keep):
    steps = u_ref.shape[0] // SUBLANES
    for pack in packs:
        _, column, _, width, _ = pack
        cols = slice(column, column + width)
        for direction in range(2):
            fill_pack(pack, direction, channels, u_ref, in_ref, keep_ref, push_re, push_im, keep)
            rate_re = rate_ref[2 * direction : 2 * direction + 1, cols]
            rate_im = rate_ref[2 * direction + 1 : 2 * direction + 2, cols]
            h_re = jnp.zeros((SUBLANES, width), jnp.float32)
            h_im = jnp.zeros((SUBLANES, width), jnp.float32)
            kept = jnp.ones((SUBLANES, width), jnp.float32)
            for step in order(steps, direction):
                rows = slice(step * SUBLANES, (step + 1) * SUBLANES)
                hold = keep[rows, :width]
                new_re = hold * (rate_re * h_re - rate_im * h_im) + push_re[rows, :width]
                h_im = hold * (rate_re * h_im + rate_im * h_re) + push_im[rows, :width]
                h_re = new_re
                kept = kept * hold
            power_re, power_im = complex_power(rate_re, rate_im, steps)
            sub_ref[direction, 0, :, cols] = h_re
            sub_ref[direction, 1, :, cols] = h_im
            sub_ref[direction, 2, :, cols] = kept * power_re
            sub_ref[direction, 3, :, cols] = kept * power_im
            decay_re = kept * power_re
            decay_im = kept * power_im
            e_re = jnp.zeros((1, width), jnp.float32)
            e_im = jnp.zeros((1, width), jnp.float32)
            t_re = jnp.ones((1, width), jnp.float32)
            t_im = jnp.zeros((1, width), jnp.float32)
            for j in order(SUBLANES, direction):
                d_re, d_im = decay_re[j : j + 1], decay_im[j : j + 1]
                e_re, e_im = (
                    d_re * e_re - d_im * e_im + h_re[j : j + 1],
                    d_re * e_im + d_im * e_re + h_im[j : j + 1],
                )
                t_re, t_im = d_re * t_re - d_im * t_im, d_re * t_im + d_im * t_re
            for part, value in enumerate((e_re, e_im, t_re, t_im)):
                row = 4 * direction + part
                ends_ref[row : row + 1, cols] = value


def mix_kernel(
    packs, channels, u_ref, in_ref, rate_ref, keep_ref, sub_ref, all_ref, out_map_ref, skip_ref,
    gate_ref, out_ref, push_re, push_im, keep, carry,
):
    tokens = u_ref.shape[0]
    steps = tokens // SUBLANES
    count = all_ref.shape[0]
    mine = lax.axis_index("sp")
    total_width = all_ref.shape[2]

    def hop(k, state):
        result = []
        for direction in range(2):
            at = k if direction == 0 else count - 1 - k
            use = at < mine if direction == 0 else at > mine
            c_re, c_im = state[2 * direction], state[2 * direction + 1]
            base = 4 * direction
            e_re = all_ref[at, base : base + 1, :]
            e_im = all_ref[at, base + 1 : base + 2, :]
            d_re = all_ref[at, base + 2 : base + 3, :]
            d_im = all_ref[at, base + 3 : base + 4, :]
            result.append(jnp.where(use, d_re * c_re - d_im * c_im + e_re, c_re))
            result.append(jnp.where(use, d_re * c_im + d_im * c_re + e_im, c_im))
        return tuple(result)

    zero = jnp.zeros((1, total_width), jnp.float32)
    entering = lax.fori_loop(0, count, hop, (zero, zero, zero, zero))
    for direction in range(2):
        c_re, c_im = entering[2 * direction], entering[2 * direction + 1]
        for j in order(SUBLANES, direction):
            carry[direction, 0, j : j + 1, :] = c_re
            carry[direction, 1, j : j + 1, :] = c_im
            d_re = sub_ref[direction, 2, j : j + 1, :]
            d_im = sub_ref[direction, 3, j : j + 1, :]
            c_re, c_im = (
                d_re * c_re - d_im * c_im + sub_ref[direction, 0, j : j + 1, :],
                d_re * c_im + d_im * c_re + sub_ref[direction, 1, j : j + 1, :],
            )
    for pack in packs:
        channel, column, _, width, states = pack
        cols = slice(column, column + width)
        lanes = slice(channel, channel + LANES)
        read = None
        for direction in range(2):
            fill_pack(pack, direction, channels, u_ref, in_ref, keep_ref, push_re, push_im, keep)
            rate_re = rate_ref[2 * direction : 2 * direction + 1, cols]
            rate_im = rate_ref[2 * direction + 1 : 2 * direction + 2, cols]
            h_re = carry[direction, 0, :, cols]
            h_im = carry[direction, 1, :, cols]
            for step in order(steps, direction):
                rows = slice(step * SUBLANES, (step + 1) * SUBLANES)
                hold = keep[rows, :width]
                new_re = hold * (rate_re * h_re - rate_im * h_im) + push_re[rows, :width]
                h_im = hold * (rate_re * h_im + rate_im * h_re) + push_im[rows, :width]
                h_re = new_re
                push_re[rows, :width] = h_re
                push_im[rows, :width] = h_im
            for part, source in enumerate((push_re, push_im)):
                rows = out_map_ref[direction, part, :, cols]
                if part:
                    rows = -rows
                term = lax.dot_general(
                    source[:, :width].astype(jnp.bfloat16),
                    spread(rows, channels, states),
                    (((1,), (1,)), ((), ())),
                    preferred_element_type=jnp.float32,
                )
                read = term if read is None else read + term
        shaped = read + skip_ref[:, lanes] * u_ref[:, lanes].astype(jnp.float32)
        active = jax.nn.gelu(shaped, approximate=True)
        gate = spread(gate_ref[:, lanes], channels, channels)
        opened = jax.nn.sigmoid(
            jnp.dot(active.astype(jnp.bfloat16), gate, preferred_element_type=jnp.float32)
        )
        out_ref[:, lanes] = (active * opened).astype(jnp.bfloat16)


def share_kernel(ends_ref, all_ref, send_sem, recv_sem):
    count = lax.axis_size("sp")
    mine = lax.axis_index("sp")
    barrier = pltpu.get_barrier_semaphore()
    for k in range(1, count):
        pl.semaphore_signal(
            barrier,
            inc=1,
            device_id={"sp": lax.rem(mine + k, count)},
            device_id_type=pl.DeviceIdType.MESH,
        )
    pl.semaphore_wait(barrier, count - 1)
    copies = []
    for k in range(1, count):
        copy = pltpu.make_async_remote_copy(
            src_ref=ends_ref,
            dst_ref=all_ref.at[mine],
            send_sem=send_sem.at[k],
            recv_sem=recv_sem.at[k],
            device_id={"sp": lax.rem(mine + k, count)},
            device_id_type=pl.DeviceIdType.MESH,
        )
        copy.start()
        copies.append(copy)
    all_ref[mine] = ends_ref[...]
    for copy in copies:
        copy.wait()


def share_ends(ends):
    count = lax.axis_size("sp")
    vmem = pl.BlockSpec(memory_space=pltpu.VMEM)
    return pl.pallas_call(
        share_kernel,
        out_shape=jax.ShapeDtypeStruct((count,) + ends.shape, ends.dtype),
        in_specs=[vmem],
        out_specs=vmem,
        scratch_shapes=[pltpu.SemaphoreType.DMA((count,)), pltpu.SemaphoreType.DMA((count,))],
        compiler_params=pltpu.CompilerParams(collective_id=0, has_side_effects=True),
        name="share_ends",
    )(ends)


def entering_map(poles, step, in_map):
    re, im = poles[:, 0], poles[:, 1]
    growth = jnp.exp(re)
    rate = jnp.stack([growth * jnp.cos(im), growth * jnp.sin(im)], axis=1)
    numer_re = rate[:, 0] - 1.0
    numer_im = rate[:, 1]
    denom = re * re + im * im
    factor_re = ((numer_re * re + numer_im * im) / denom * step[:, :, None])[:, None]
    factor_im = ((numer_im * re - numer_re * im) / denom * step[:, :, None])[:, None]
    moved = jnp.transpose(in_map, (0, 1, 3, 2, 4))
    enter = jnp.stack(
        [
            factor_re * moved[:, 0] - factor_im * moved[:, 1],
            factor_re * moved[:, 1] + factor_im * moved[:, 0],
        ],
        axis=1,
    )
    return rate.reshape(4, -1), enter.reshape(enter.shape[:3] + (-1,))


def mixer(
    wide_inputs, narrow_inputs, wide_poles, narrow_poles, step_sizes, forget, wide_in_map,
    narrow_in_map, wide_out_map, narrow_out_map, skip_weight, gate_mix,
):
    tokens, width = wide_inputs.shape
    groups, channels, wide_state = wide_in_map.shape[2:]
    narrow_state = narrow_in_map.shape[4]
    packs = packs_of(channels, groups, wide_state, narrow_state)
    steps = tokens // SUBLANES
    total = groups * (wide_state + narrow_state)
    widest = max(pack[3] for pack in packs)

    def weave(rows):
        return jnp.swapaxes(rows.reshape(SUBLANES, steps, -1), 0, 1).reshape(tokens, -1)

    signal = weave(jnp.concatenate([wide_inputs, narrow_inputs], axis=1))
    held = jnp.exp(-forget).reshape(2, 2 * groups, SUBLANES, steps)
    held = jnp.transpose(held, (0, 3, 2, 1)).reshape(2, tokens, 2 * groups)
    wide_rate, wide_enter = entering_map(wide_poles, step_sizes[:, 0], wide_in_map)
    narrow_rate, narrow_enter = entering_map(narrow_poles, step_sizes[:, 1], narrow_in_map)
    rate = jnp.concatenate([wide_rate, narrow_rate], axis=1)
    enter = jnp.concatenate([wide_enter, narrow_enter], axis=3)
    leave = jnp.concatenate(
        [
            jnp.transpose(each, (0, 1, 3, 2, 4)).reshape(2, 2, channels, -1)
            for each in (wide_out_map, narrow_out_map)
        ],
        axis=3,
    )
    skip = skip_weight.astype(jnp.float32).reshape(1, -1)
    gate = jnp.transpose(gate_mix.astype(jnp.float32), (2, 0, 1, 3)).reshape(channels, -1)
    vmem = pl.BlockSpec(memory_space=pltpu.VMEM)
    scratch = [pltpu.VMEM((tokens, widest), jnp.float32) for _ in range(3)]
    ends, sub = pl.pallas_call(
        functools.partial(ends_kernel, packs, channels),
        out_shape=(
            jax.ShapeDtypeStruct((8, total), jnp.float32),
            jax.ShapeDtypeStruct((2, 4, SUBLANES, total), jnp.float32),
        ),
        in_specs=[vmem] * 4,
        out_specs=(vmem, vmem),
        scratch_shapes=scratch,
        name="ends",
    )(signal, enter, rate, held)
    gathered = share_ends(ends)
    mixed = pl.pallas_call(
        functools.partial(mix_kernel, packs, channels),
        out_shape=jax.ShapeDtypeStruct((tokens, 2 * width), jnp.bfloat16),
        in_specs=[vmem] * 9,
        out_specs=vmem,
        scratch_shapes=scratch + [pltpu.VMEM((2, 2, SUBLANES, total), jnp.float32)],
        name="mix",
    )(signal, enter, rate, held, sub, gathered, leave, skip, gate)
    return jnp.swapaxes(mixed.reshape(steps, SUBLANES, -1), 0, 1).reshape(tokens, -1)


def local(
    wide_inputs, narrow_inputs, wide_poles, narrow_poles, step_sizes, forget, wide_in_map,
    narrow_in_map, wide_out_map, narrow_out_map, skip_weight, gate_mix, residual, mixer_gain,
    out_proj, ffn_gain, routes, route_weights, gate_proj, up_proj, down_proj,
):
    n_sp = lax.axis_size("sp")
    n_tp = lax.axis_size("tp")
    tp = lax.axis_index("tp")
    set_out = mixer(
        wide_inputs, narrow_inputs, wide_poles, narrow_poles, step_sizes, forget, wide_in_map,
        narrow_in_map, wide_out_map, narrow_out_map, skip_weight, gate_mix,
    )
    tokens = set_out.shape[0]
    rows = tokens // n_tp
    half = set_out.shape[1] // 2
    swapped = lax.all_to_all(
        set_out.reshape(n_tp, rows, -1), "tp", split_axis=0, concat_axis=0, tiled=True
    )
    joined = jnp.concatenate(
        [swapped[k, :, :half] for k in range(n_tp)] + [swapped[k, :, half:] for k in range(n_tp)],
        axis=1,
    ).astype(jnp.float32)
    scale = lax.rsqrt(jnp.mean(joined * joined, axis=1, keepdims=True) + epsilon)
    mixed = (joined * scale * mixer_gain).astype(jnp.bfloat16)
    projected = jnp.dot(mixed, out_proj, preferred_element_type=jnp.float32)
    hidden1 = (residual.astype(jnp.float32) + projected).astype(jnp.bfloat16)
    hidden_wide = hidden1.astype(jnp.float32)
    normed = (
        hidden_wide
        * lax.rsqrt(jnp.mean(hidden_wide * hidden_wide, axis=1, keepdims=True) + epsilon)
        * ffn_gain
    ).astype(jnp.bfloat16)

    experts = n_sp * n_tp
    capacity = 4 * tokens // (n_tp * experts)
    top_count = routes.shape[1]
    width = normed.shape[1]
    slots = experts * capacity
    picks = routes.reshape(-1)
    entries = picks.shape[0]
    onehot = (picks[:, None] == jnp.arange(experts, dtype=jnp.int32)[None, :]).astype(jnp.bfloat16)
    earlier = (
        jnp.arange(entries)[None, :] < jnp.arange(entries)[:, None]
    ).astype(jnp.bfloat16)
    before = jnp.dot(earlier, onehot, preferred_element_type=jnp.float32)
    rank = jnp.sum(before * onehot.astype(jnp.float32), axis=1).astype(jnp.int32)
    place = (picks * capacity + rank).reshape(-1, top_count)
    hit = place[:, :, None] == jnp.arange(slots, dtype=jnp.int32)[None, None, :]
    share = route_weights / jnp.sum(route_weights, axis=1, keepdims=True)
    spot = jnp.any(hit, axis=1).astype(jnp.bfloat16)
    weight = jnp.sum(jnp.where(hit, share[:, :, None], 0.0), axis=1)
    high = lax.reduce_precision(weight, 8, 7)
    weights = jnp.concatenate([high, weight - high], axis=0).astype(jnp.bfloat16)

    sectioning = lax.dot_general(
        spot, normed, (((0,), (0,)), ((), ())), preferred_element_type=jnp.float32
    ).astype(jnp.bfloat16)
    received = lax.all_to_all(
        sectioning.reshape(experts, capacity, width),
        ("sp", "tp"),
        split_axis=0,
        concat_axis=0,
        tiled=True,
    )
    flat_rows = received.reshape(-1, width)
    gate_val = jnp.dot(flat_rows, gate_proj[0], preferred_element_type=jnp.float32)
    up_val = jnp.dot(flat_rows, up_proj[0], preferred_element_type=jnp.float32)
    expert_hidden = (jax.nn.silu(gate_val) * up_val).astype(jnp.bfloat16)
    done = jnp.dot(expert_hidden, down_proj[0], preferred_element_type=jnp.float32).astype(
        jnp.bfloat16
    )
    returned = lax.all_to_all(
        done.reshape(received.shape), ("sp", "tp"), split_axis=0, concat_axis=0, tiled=True
    )
    summed = jnp.dot(weights, returned.reshape(-1, width), preferred_element_type=jnp.float32)
    own = residual.shape[0]
    return (hidden_wide + (summed[:own] + summed[own:])).astype(jnp.bfloat16)


def solution(mesh):
    return jax.shard_map(
        local,
        mesh=mesh,
        in_specs=(
            P("sp", "tp"),
            P("sp", "tp"),
            P(None, None, "tp", None),
            P(None, None, "tp", None),
            P(None, None, "tp"),
            P(None, None, "tp", "sp"),
            P(None, None, "tp", None, None),
            P(None, None, "tp", None, None),
            P(None, None, "tp", None, None),
            P(None, None, "tp", None, None),
            P(None, "tp"),
            P(None, "tp", None, None),
            P(("sp", "tp"), None),
            P(),
            P(),
            P(),
            P(("sp", "tp"), None),
            P(("sp", "tp"), None),
            P(("sp", "tp"), None, None),
            P(("sp", "tp"), None, None),
            P(("sp", "tp"), None, None),
        ),
        out_specs=P(("sp", "tp"), None),
        check_vma=False,
    )
```

profile of v0, /device:TPU:9, one launch (start us, length us, event | category | flops | bytes accessed | tf_op | source)
XLA Modules:
  0.0 132.3 jit_solution(16091675669083835766)
XLA Ops:
  0.0 0.8 fusion.51
  0.8 0.8 multiply_bitcast_fusion.3
  1.6 0.8 multiply_bitcast_fusion.2
  2.4 0.8 multiply_bitcast_fusion.1
  3.3 0.8 multiply_bitcast_fusion
  4.1 1.1 multiply_subtract_fusion.1
  5.7 1.1 multiply_subtract_fusion
  6.8 0.1 stack.31
  7.2 0.2 copy.69
  7.4 0.2 reshape.93
  7.6 0.2 copy.70
  7.8 0.2 reshape.94
  8.3 0.8 copy.68
  9.2 0.7 copy.77
  9.9 1.0 maximum_maximum_fusion
  10.9 4.0 %ends.1 = (f32[8,1536]{1,0:T(8,128)}, f32[2,4,8,1536]{3,2,1,0:T(8,128)}) custom-call(bf16[128,512]{1,0:T(8,128)(2,1)} %bitcast.105, f32[2,2,16,1536]{3,2,1,0:T(8,128)} %get-tuple-element.29.in_ref, f32[4,1536]{1,0:T(4,128)} %copy-done.3, f32[2,128,32]{2,1,0:T(8,128)} %bitcast.103), custom_call_target="tpu_custom_call" | custom-call | tf_op jit(solution)/shard_map/ends/pallas_call | solution.py:284
  14.9 22.4 %share_ends.1.all_ref = f32[16,8,1536]{2,1,0:T(8,128)} custom-call(f32[8,1536]{1,0:T(8,128)} %get-tuple-element.8.ends_ref), custom_call_target="tpu_custom_call" | custom-call | tf_op jit(solution)/shard_map/share_ends/pallas_call | solution.py:220
  37.4 0.8 reshape.107.gate_ref
  38.2 0.6 copy.75
  38.8 6.8 %mix.1 = bf16[128,512]{1,0:T(8,128)(2,1)} custom-call(bf16[128,512]{1,0:T(8,128)(2,1)} %bitcast.106, f32[2,2,16,1536]{3,2,1,0:T(8,128)} %get-tuple-element.29.in_ref, f32[4,1536]{1,0:T(4,128)} %copy-done.3, f32[2,128,32]{2,1,0:T(8,128)} %bitcast.104, f32[2,4,8,1536]{3,2,1,0:T(8,128)} %get-tuple-element.7.sub_ref, f32[16,8,1536]{2,1,0:T(8,128)} %share_ends.1.all_ref, ...), custom_call_target="tpu_custom_call" | custom-call | tf_op jit(solution)/shard_map/mix/pallas_call | solution.py:296
  45.5 0.9 copy.72
  46.5 5.0 %all_to_all.15 = bf16[2,64,512]{2,1,0:T(8,128)(2,1)S(1)} all-to-all(bf16[2,64,512]{2,1,0:T(8,128)(2,1)S(1)} %bitcast.113), channel_id=1, replica_groups=mesh['sp'=16,'tp'=2] {'tp'}, dimensions={0} | all-to-all | bytes 262144 | tf_op jit(solution)/shard_map/all_to_all | solution.py:322
  51.7 3.2 %multiply_reduce_fusion = (f32[64]{0:T(128)S(1)}, f32[64,2048]{1,0:T(8,128)S(1)}) fusion(bf16[1024,2048]{1,0:T(8,128)(2,1)} %param.35, f32[1024]{0:T(1024)S(1)} %copy-done.9, f32[64]{0:T(128)S(1)} %add_rsqrt_fusion.1, bf16[64,256]{1,0:T(8,128)(2,1)S(1)} %get-tuple-element.20, bf16[64,256]{1,0:T(8,128)(2,1)S(1)} %get-tuple-element.21, ...), kind=kOutput, calls=%fused_computation.26 | convolution fusion | flops 269942720 | bytes 5116416 | tf_op jit(solution)/shard_map/dot_general | solution.py:331
  55.2 0.2 fusion.21
  55.7 0.5 fusion.15
  56.2 31.8 %all_to_all.16 = bf16[32,8,2048]{2,1,0:T(8,128)(2,1)S(1)} all-to-all(bf16[32,8,2048]{2,1,0:T(8,128)(2,1)S(1)} %fusion.15), channel_id=1, replica_groups=mesh['sp'=16,'tp'=2] {'sp','tp'}, dimensions={0} | all-to-all | bytes 2097152 | tf_op jit(solution)/shard_map/all_to_all | solution.py:364
  88.0 4.5 %fusion.4 = f32[256,1408]{1,0:T(8,128)S(1)} fusion(bf16[1,2048,1408]{2,1,0:T(8,128)(2,1)} %param.39, bf16[32,8,2048]{2,1,0:T(8,128)(2,1)S(1)} %all_to_all.16), kind=kOutput, calls=%fused_computation.4 | convolution fusion | flops 1476395008 | bytes 8257536 | tf_op jit(solution)/shard_map/dot_general | solution.py:372
  92.5 8.9 %fusion.16 = bf16[32,8,2048]{2,1,0:T(8,128)(2,1)} fusion(bf16[1,1408,2048]{2,1,0:T(8,128)(2,1)} %param.41, bf16[1,2048,1408]{2,1,0:T(8,128)(2,1)} %param.40, f32[256,1408]{1,0:T(8,128)S(1)} %fusion.4, bf16[32,8,2048]{2,1,0:T(8,128)(2,1)S(1)} %all_to_all.16), kind=kOutput, calls=%fused_computation.11 | convolution fusion | flops 2955476992 | bytes 15073280 | tf_op jit(solution)/shard_map/dot_general | solution.py:375
  101.4 4.5 %all-to-all-start.2 = ((bf16[32,8,2048]{2,1,0:T(8,128)(2,1)}), bf16[32,8,2048]{2,1,0:T(8,128)(2,1)S(1)}, u32[]{:S(2)}, u32[]{:S(2)}) async-start(bf16[32,8,2048]{2,1,0:T(8,128)(2,1)} %fusion.16), calls=%async_computation.2 | async-start | bytes 2097152 | tf_op jit(solution)/shard_map/all_to_all | solution.py:378
  106.1 25.1 %all-to-all-done.2 = bf16[32,8,2048]{2,1,0:T(8,128)(2,1)S(1)} async-done(((bf16[32,8,2048]{2,1,0:T(8,128)(2,1)}), bf16[32,8,2048]{2,1,0:T(8,128)(2,1)S(1)}, u32[]{:S(2)}, u32[]{:S(2)}) %all-to-all-start.2) | async-done | bytes 1048608 | tf_op jit(solution)/shard_map/all_to_all | solution.py:378
  131.2 0.3 fusion.22
  131.5 0.8 fusion.32
  (60 shorter events, 2.1 us)
Async XLA Ops:
  0.0 7.2 %copy-start = (f32[2,2,16,16,64]{4,3,2,1,0:T(8,128)S(1)}, f32[2,2,16,16,64]{4,3,2,1,0:T(8,128)}, u32[]{:S(2)}) copy-start(f32[2,2,16,16,64]{4,3,2,1,0:T(8,128)} %param.29) | copy-start | bytes 786436
  0.0 7.6 %copy-start.1 = (f32[2,2,16,16,32]{4,3,2,1,0:T(8,128)S(1)}, f32[2,2,16,16,32]{4,3,2,1,0:T(8,128)}, u32[]{:S(2)}) copy-start(f32[2,2,16,16,32]{4,3,2,1,0:T(8,128)} %param.30) | copy-start | bytes 393220
  5.2 3.0 %copy-start.7 = (f32[2,2,16,128]{3,2,1,0:T(8,128)S(1)}, f32[2,2,16,128]{3,2,1,0:T(8,128)}, u32[]{:S(2)}) copy-start(f32[2,2,16,128]{3,2,1,0:T(8,128)} %param.26) | copy-start | bytes 98308
  5.3 3.8 %copy-start.5 = (bf16[128,256]{1,0:T(8,128)(2,1)S(1)}, bf16[128,256]{1,0:T(8,128)(2,1)}, u32[]{:S(2)}) copy-start(bf16[128,256]{1,0:T(8,128)(2,1)} %param.22) | copy-start | bytes 196612
  5.3 3.8 %copy-start.6 = (bf16[128,256]{1,0:T(8,128)(2,1)S(1)}, bf16[128,256]{1,0:T(8,128)(2,1)}, u32[]{:S(2)}) copy-start(bf16[128,256]{1,0:T(8,128)(2,1)} %param.21) | copy-start | bytes 196612
  7.1 30.2 %copy-start.4 = (bf16[2,16,16,16]{3,2,1,0:T(8,128)(2,1)S(1)}, bf16[2,16,16,16]{3,2,1,0:T(8,128)(2,1)}, u32[]{:S(2)}) copy-start(bf16[2,16,16,16]{3,2,1,0:T(8,128)(2,1)} %param.32) | copy-start | bytes 49156
  7.4 30.8 %copy-start.12 = (bf16[2,256]{1,0:T(2,128)(2,1)S(1)}, bf16[2,256]{1,0:T(2,128)(2,1)}, u32[]{:S(2)}) copy-start(bf16[2,256]{1,0:T(2,128)(2,1)} %param.31) | copy-start | bytes 3076
  9.1 42.5 %copy-start.2 = (bf16[64,2048]{1,0:T(8,128)(2,1)S(1)}, bf16[64,2048]{1,0:T(8,128)(2,1)}, u32[]{:S(2)}) copy-start(bf16[64,2048]{1,0:T(8,128)(2,1)} %param.33) | copy-start | bytes 786436
  9.1 42.5 %copy-start.9 = (f32[1024]{0:T(1024)S(1)}, f32[1024]{0:T(1024)}, u32[]{:S(2)}) copy-start(f32[1024]{0:T(1024)} %param.34) | copy-start | bytes 12292
  9.9 1.0 copy-start.3
  38.8 16.2 %copy-start.10 = (s32[64,2]{0,1:T(2,128)S(1)}, s32[64,2]{0,1:T(2,128)}, u32[]{:S(2)}) copy-start(s32[64,2]{0,1:T(2,128)} %param.37) | copy-start | bytes 1540
  38.8 16.9 %copy-start.8 = (f32[2048]{0:T(1024)S(1)}, f32[2048]{0:T(1024)}, u32[]{:S(2)}) copy-start(f32[2048]{0:T(1024)} %param.36) | copy-start | bytes 24580
  92.5 13.5 %copy-start.11 = (f32[64,2]{0,1:T(2,128)S(1)}, f32[64,2]{0,1:T(2,128)}, u32[]{:S(2)}) copy-start(f32[64,2]{0,1:T(2,128)} %param.38) | copy-start | bytes 1540
  101.4 29.8 %all-to-all-start.2 = ((bf16[32,8,2048]{2,1,0:T(8,128)(2,1)}), bf16[32,8,2048]{2,1,0:T(8,128)(2,1)S(1)}, u32[]{:S(2)}, u32[]{:S(2)}) async-start(bf16[32,8,2048]{2,1,0:T(8,128)(2,1)} %fusion.16), calls=%async_computation.2 | async-start | bytes 2097152 | tf_op jit(solution)/shard_map/all_to_all | solution.py:378
where the time goes:
time: 135 us; the launch traced here: 132 us
  blocking collectives  36.8 us (27%)
  Pallas kernels  33.2 us (25%)
  waiting for transfers between devices  25.1 us (19%)
  matrix products  17.5 us (13%)
  other arithmetic  7.71 us (6%)
  local copies, waits for them, and re-layouts  7.11 us (5%)
  starting transfers between devices  4.54 us (3%)
    all_to_all x1, blocking collectives, local(): lax.all_to_all(sectioning.reshape(experts, capacity, width), ('sp', 'tp')...  31.8 us
    all_to_all x1, waiting for transfers between devices, local(): lax.all_to_all(done.reshape(received.shape), ('sp', 'tp'), split_axis=0,...  25.1 us
    pallas_call x1, Pallas kernels, share_ends(): pl.pallas_call(share_kernel, out_shape=jax.ShapeDtypeStruct((count,) + en...  22.4 us
    dot_general x1, matrix products, local(): jnp.dot(expert_hidden, down_proj[0], preferred_element_type=jnp.float32)  8.89 us
    pallas_call x1, Pallas kernels, mixer(): pl.pallas_call(functools.partial(mix_kernel, packs, channels), out_shape=...  6.79 us
    all_to_all x1, blocking collectives, local(): lax.all_to_all(set_out.reshape(n_tp, rows, -1), 'tp', split_axis=0, conca...  5.02 us
    all_to_all x1, starting transfers between devices, local(): lax.all_to_all(done.reshape(received.shape), ('sp', 'tp'), split_axis=0,...  4.54 us
    dot_general x1, matrix products, local(): jnp.dot(flat_rows, gate_proj[0], preferred_element_type=jnp.float32)  4.45 us
  transfers between devices with their start and end apart: 1, of which 1 were waited for; matrix products, arithmetic and copies ran while one was open for 0% of the time, Pallas kernels for 0%

commit v1 on v0

v1 whole, which is shorter than its diff:
```python
import jax
import jax.numpy as jnp
from jax import lax
from jax.experimental import pallas as pl
from jax.experimental.pallas import tpu as pltpu
from jax.sharding import PartitionSpec as P

epsilon = 1e-06
SUBLANES = 8
LANES = 128


def complex_power(re, im, exponent):
    out_re, out_im = None, None
    while exponent:
        if exponent & 1:
            if out_re is None:
                out_re, out_im = re, im
            else:
                out_re, out_im = out_re * re - out_im * im, out_re * im + out_im * re
        re, im = re * re - im * im, 2.0 * re * im
        exponent >>= 1
    return out_re, out_im


def pack_list(channels, groups, sets):
    per = LANES // channels
    packs, column = [], 0
    for which, states in enumerate(sets):
        for pack in range(groups // per):
            packs.append((which, pack, column, per * states, states))
            column += per * states
    return packs, column


def order(count, direction):
    return range(count) if direction == 0 else range(count - 1, -1, -1)


def widen(rows, copies):
    return jnp.concatenate([rows] * copies, axis=1)


def block_diagonal(rows, channels, states):
    copies = LANES // channels
    tiled = widen(rows, copies)
    row = lax.broadcasted_iota(jnp.int32, tiled.shape, 0) // channels
    column = lax.broadcasted_iota(jnp.int32, tiled.shape, 1) // states
    return jnp.where(row == column, tiled, 0.0).astype(jnp.bfloat16)


def flat_row(rows, states):
    copies = rows.shape[0]
    tiled = widen(rows, copies)
    row = lax.broadcasted_iota(jnp.int32, tiled.shape, 0)
    column = lax.broadcasted_iota(jnp.int32, tiled.shape, 1) // states
    return jnp.sum(jnp.where(row == column, tiled, 0.0), axis=0, keepdims=True)


def split3(value):
    high = value.astype(jnp.bfloat16)
    rest = value - high.astype(jnp.float32)
    mid = rest.astype(jnp.bfloat16)
    low = (rest - mid.astype(jnp.float32)).astype(jnp.bfloat16)
    return high, mid, low


def owners(pack, groups, count, channels):
    which, number, _, width, states = pack
    first = which * groups + number * (LANES // channels)
    row = lax.broadcasted_iota(jnp.int32, (3 * count, width), 0) % count
    column = first + lax.broadcasted_iota(jnp.int32, (3 * count, width), 1) // states
    return jnp.where(row == column, 1.0, 0.0).astype(jnp.bfloat16)


def mixer_kernel(
    wide_u, narrow_u, wide_poles, narrow_poles, step_ref, forget_ref, wide_in, narrow_in,
    wide_out, narrow_out, skip_ref, gate_ref, out_ref,
    signal, push, keep, ends_ref, sub_ref, all_ref, carry, mixed, send_sem, recv_sem, swap_sem,
):
    tokens, half = wide_u.shape
    groups, channels = wide_in.shape[2:4]
    sets = (wide_in.shape[4], narrow_in.shape[4])
    packs, total = pack_list(channels, groups, sets)
    per = LANES // channels
    steps = tokens // SUBLANES
    span = ends_ref.shape[2]
    count = lax.axis_size("sp")
    n_tp = lax.axis_size("tp")
    mine = lax.axis_index("sp")
    tp = lax.axis_index("tp")
    barrier = pltpu.get_barrier_semaphore()
    for k in range(1, count):
        pl.semaphore_signal(
            barrier, inc=1, device_id={"sp": lax.rem(mine + k, count)},
            device_id_type=pl.DeviceIdType.MESH,
        )
    for k in range(1, n_tp):
        pl.semaphore_signal(
            barrier, inc=1, device_id={"tp": lax.rem(tp + k, n_tp)},
            device_id_type=pl.DeviceIdType.MESH,
        )

    row = lax.broadcasted_iota(jnp.int32, (tokens, tokens), 0)
    column = lax.broadcasted_iota(jnp.int32, (tokens, tokens), 1)
    weave = jnp.where(
        column == (row % SUBLANES) * steps + row // SUBLANES, 1.0, 0.0
    ).astype(jnp.bfloat16)
    unweave = jnp.where(
        row == (column % SUBLANES) * steps + column // SUBLANES, 1.0, 0.0
    ).astype(jnp.bfloat16)
    inputs = (wide_u, narrow_u)
    for which in range(2):
        signal[:, which * half : (which + 1) * half] = jnp.dot(
            weave, inputs[which][...], preferred_element_type=jnp.float32
        ).astype(jnp.bfloat16)
    held = []
    n_groups = 2 * groups
    for direction in range(2):
        rows = jnp.concatenate([forget_ref[direction, 0], forget_ref[direction, 1]], axis=0)
        pieces = jnp.concatenate(split3(jnp.exp(-rows)), axis=0)
        held.append(
            lax.dot_general(
                weave, pieces, (((1,), (1,)), ((), ())), preferred_element_type=jnp.float32
            ).astype(jnp.bfloat16)
        )
        sums = lax.dot_general(
            jnp.ones((SUBLANES, tokens), jnp.float32), rows, (((1,), (1,)), ((), ())),
            precision=lax.Precision.HIGHEST, preferred_element_type=jnp.float32,
        )
        ends_ref[direction, 6:8, :] = jnp.zeros((2, span), jnp.float32)
        ends_ref[direction, 6:7, :n_groups] = jnp.exp(-sums[:1])

    def put(direction, part, column, value):
        done = 0
        while done < value.shape[1]:
            at = column + done
            line, start = at // span, at % span
            size = min(value.shape[1] - done, span - start)
            ends_ref[direction, 3 * part + line : 3 * part + line + 1, start : start + size] = (
                value[:, done : done + size]
            )
            done += size

    eye_row = lax.broadcasted_iota(jnp.int32, (per, groups), 0)
    eye_column = lax.broadcasted_iota(jnp.int32, (per, groups), 1)
    poles, in_maps = (wide_poles, narrow_poles), (wide_in, narrow_in)
    rates = {}
    for pack in packs:
        which, number, column, width, states = pack
        cols = slice(column, column + width)
        at = slice(number * per, (number + 1) * per)
        lanes = slice(which * half + number * LANES, which * half + (number + 1) * LANES)
        owner = owners(pack, groups, n_groups, channels)
        for direction in range(2):
            re, im = poles[which][direction, 0, at, :], poles[which][direction, 1, at, :]
            growth = jnp.exp(re)
            rate_re, rate_im = growth * jnp.cos(im), growth * jnp.sin(im)
            numer = rate_re - 1.0
            step = jnp.sum(
                jnp.where(
                    eye_column == eye_row + number * per,
                    step_ref[direction, which : which + 1, :], 0.0,
                ),
                axis=1, keepdims=True,
            )
            scale = step / (re * re + im * im)
            factor_re = ((numer * re + rate_im * im) * scale)[:, None, :]
            factor_im = ((rate_im * re - numer * im) * scale)[:, None, :]
            in_re, in_im = in_maps[which][direction, 0, at], in_maps[which][direction, 1, at]
            enter = (factor_re * in_re - factor_im * in_im, factor_re * in_im + factor_im * in_re)
            for part in range(2):
                push[direction, part, :, cols] = jnp.dot(
                    signal[:, lanes],
                    block_diagonal(enter[part].reshape(LANES, states), channels, states),
                    preferred_element_type=jnp.float32,
                )
            keep[direction, :, cols] = jnp.dot(
                held[direction], owner, preferred_element_type=jnp.float32
            )
            rate_re, rate_im = flat_row(rate_re, states), flat_row(rate_im, states)
            rates[direction, column] = (rate_re, rate_im)
            h_re = jnp.zeros((SUBLANES, width), jnp.float32)
            h_im = jnp.zeros((SUBLANES, width), jnp.float32)
            kept = jnp.ones((SUBLANES, width), jnp.float32)
            for step in order(steps, direction):
                rows = slice(step * SUBLANES, (step + 1) * SUBLANES)
                hold = keep[direction, rows, cols]
                new_re = hold * (rate_re * h_re - rate_im * h_im) + push[direction, 0, rows, cols]
                h_im = hold * (rate_re * h_im + rate_im * h_re) + push[direction, 1, rows, cols]
                h_re = new_re
                kept = kept * hold
            power_re, power_im = complex_power(rate_re, rate_im, steps)
            decay_re, decay_im = kept * power_re, kept * power_im
            for part, value in enumerate((h_re, h_im, decay_re, decay_im)):
                sub_ref[direction, part, :, cols] = value
            e_re = jnp.zeros((1, width), jnp.float32)
            e_im = jnp.zeros((1, width), jnp.float32)
            for j in order(SUBLANES, direction):
                d_re, d_im = decay_re[j : j + 1], decay_im[j : j + 1]
                e_re, e_im = (
                    d_re * e_re - d_im * e_im + h_re[j : j + 1],
                    d_re * e_im + d_im * e_re + h_im[j : j + 1],
                )
            put(direction, 0, column, e_re)
            put(direction, 1, column, e_im)

    pl.semaphore_wait(barrier, count - 1 + n_tp - 1)
    copies = []
    for k in range(1, count):
        copy = pltpu.make_async_remote_copy(
            src_ref=ends_ref.at[(mine + k) // count],
            dst_ref=all_ref.at[mine],
            send_sem=send_sem.at[k],
            recv_sem=recv_sem.at[k],
            device_id={"sp": lax.rem(mine + k, count)},
            device_id_type=pl.DeviceIdType.MESH,
        )
        copy.start()
        copies.append(copy)
    all_ref[mine] = jnp.zeros(ends_ref.shape[1:], jnp.float32)
    for copy in copies:
        copy.wait()

    shares = jnp.concatenate(
        [all_ref[b, 6:7, :n_groups] for b in range(count)], axis=0
    )
    shares = jnp.concatenate(split3(shares), axis=1)
    for pack in packs:
        which, number, column, width, states = pack
        cols = slice(column, column + width)
        line, start = column // span, column % span
        kept = jnp.dot(
            shares, owners(pack, groups, n_groups, channels), preferred_element_type=jnp.float32
        )
        for direction in range(2):
            rate_re, rate_im = rates[direction, column]
            power_re, power_im = complex_power(rate_re, rate_im, tokens)
            c_re = jnp.zeros((1, width), jnp.float32)
            c_im = jnp.zeros((1, width), jnp.float32)
            for b in order(count, direction):
                use = b < mine if direction == 0 else b > mine
                e_re = all_ref[b, line : line + 1, start : start + width]
                e_im = all_ref[b, 3 + line : 4 + line, start : start + width]
                d_re, d_im = kept[b : b + 1] * power_re, kept[b : b + 1] * power_im
                c_re, c_im = (
                    jnp.where(use, d_re * c_re - d_im * c_im + e_re, c_re),
                    jnp.where(use, d_re * c_im + d_im * c_re + e_im, c_im),
                )
            for j in order(SUBLANES, direction):
                carry[direction, 0, j : j + 1, cols] = c_re
                carry[direction, 1, j : j + 1, cols] = c_im
                d_re = sub_ref[direction, 2, j : j + 1, cols]
                d_im = sub_ref[direction, 3, j : j + 1, cols]
                c_re, c_im = (
                    d_re * c_re - d_im * c_im + sub_ref[direction, 0, j : j + 1, cols],
                    d_re * c_im + d_im * c_re + sub_ref[direction, 1, j : j + 1, cols],
                )
    out_maps = (wide_out, narrow_out)
    for pack in packs:
        which, number, column, width, states = pack
        cols = slice(column, column + width)
        at = slice(number * per, (number + 1) * per)
        lanes = slice(which * half + number * LANES, which * half + (number + 1) * LANES)
        local = slice(number * LANES, (number + 1) * LANES)
        read = None
        for direction in range(2):
            rate_re, rate_im = rates[direction, column]
            h_re = carry[direction, 0, :, cols]
            h_im = carry[direction, 1, :, cols]
            for step in order(steps, direction):
                rows = slice(step * SUBLANES, (step + 1) * SUBLANES)
                hold = keep[direction, rows, cols]
                new_re = hold * (rate_re * h_re - rate_im * h_im) + push[direction, 0, rows, cols]
                h_im = hold * (rate_re * h_im + rate_im * h_re) + push[direction, 1, rows, cols]
                h_re = new_re
                push[direction, 0, rows, cols] = h_re
                push[direction, 1, rows, cols] = h_im
            for part in range(2):
                rows = out_maps[which][direction, part, at].reshape(LANES, states)
                if part:
                    rows = -rows
                term = lax.dot_general(
                    push[direction, part, :, cols].astype(jnp.bfloat16),
                    block_diagonal(rows, channels, states),
                    (((1,), (1,)), ((), ())),
                    preferred_element_type=jnp.float32,
                )
                read = term if read is None else read + term
        shaped = read + skip_ref[which : which + 1, local].astype(jnp.float32) * signal[
            :, lanes
        ].astype(jnp.float32)
        active = jax.nn.gelu(shaped, approximate=True)
        gate = block_diagonal(
            gate_ref[which, at].astype(jnp.float32).reshape(LANES, channels), channels, channels
        )
        opened = jax.nn.sigmoid(
            jnp.dot(active.astype(jnp.bfloat16), gate, preferred_element_type=jnp.float32)
        )
        mixed[:, lanes] = jnp.dot(
            unweave, (active * opened).astype(jnp.bfloat16), preferred_element_type=jnp.float32
        ).astype(jnp.bfloat16)
    rows = tokens // n_tp
    swaps = []
    for k in range(1, n_tp):
        other = lax.rem(tp + k, n_tp)
        copy = pltpu.make_async_remote_copy(
            src_ref=mixed.at[pl.ds(pl.multiple_of(other * rows, rows), rows)],
            dst_ref=out_ref.at[tp],
            send_sem=swap_sem.at[0, k],
            recv_sem=swap_sem.at[1, k],
            device_id={"tp": other},
            device_id_type=pl.DeviceIdType.MESH,
        )
        copy.start()
        swaps.append(copy)
    out_ref[tp] = mixed[pl.ds(pl.multiple_of(tp * rows, rows), rows), :]
    for copy in swaps:
        copy.wait()


def mixer(*args):
    tokens, half = args[0].shape
    groups, channels, wide_state = args[6].shape[2:]
    narrow_state = args[7].shape[4]
    _, total = pack_list(channels, groups, (wide_state, narrow_state))
    count, n_tp = lax.axis_size("sp"), lax.axis_size("tp")
    span = total // 3
    vmem = pl.BlockSpec(memory_space=pltpu.VMEM)
    return pl.pallas_call(
        mixer_kernel,
        out_shape=jax.ShapeDtypeStruct((n_tp, tokens // n_tp, 2 * half), jnp.bfloat16),
        in_specs=[vmem] * len(args),
        out_specs=vmem,
        scratch_shapes=[
            pltpu.VMEM((tokens, 2 * half), jnp.bfloat16),
            pltpu.VMEM((2, 2, tokens, total), jnp.float32),
            pltpu.VMEM((2, tokens, total), jnp.float32),
            pltpu.VMEM((2, 8, span), jnp.float32),
            pltpu.VMEM((2, 4, SUBLANES, total), jnp.float32),
            pltpu.VMEM((count, 8, span), jnp.float32),
            pltpu.VMEM((2, 2, SUBLANES, total), jnp.float32),
            pltpu.VMEM((tokens, 2 * half), jnp.bfloat16),
            pltpu.SemaphoreType.DMA((count,)),
            pltpu.SemaphoreType.DMA((count,)),
            pltpu.SemaphoreType.DMA((2, n_tp)),
        ],
        compiler_params=pltpu.CompilerParams(
            collective_id=0, has_side_effects=True, vmem_limit_bytes=24 << 20
        ),
        name="mixer",
    )(*args)


def local(
    wide_inputs, narrow_inputs, wide_poles, narrow_poles, step_sizes, forget, wide_in_map,
    narrow_in_map, wide_out_map, narrow_out_map, skip_weight, gate_mix, residual, mixer_gain,
    out_proj, ffn_gain, routes, route_weights, gate_proj, up_proj, down_proj,
):
    n_sp = lax.axis_size("sp")
    n_tp = lax.axis_size("tp")
    set_out = mixer(
        wide_inputs, narrow_inputs, wide_poles, narrow_poles, step_sizes, forget, wide_in_map,
        narrow_in_map, wide_out_map, narrow_out_map, skip_weight, gate_mix,
    )
    swapped = set_out
    rows = swapped.shape[1]
    tokens = rows * n_tp
    half = set_out.shape[2] // 2
    joined = jnp.concatenate(
        [swapped[k, :, :half] for k in range(n_tp)] + [swapped[k, :, half:] for k in range(n_tp)],
        axis=1,
    ).astype(jnp.float32)
    scale = lax.rsqrt(jnp.mean(joined * joined, axis=1, keepdims=True) + epsilon)
    mixed = (joined * scale * mixer_gain).astype(jnp.bfloat16)
    projected = jnp.dot(mixed, out_proj, preferred_element_type=jnp.float32)
    hidden1 = (residual.astype(jnp.float32) + projected).astype(jnp.bfloat16)
    hidden_wide = hidden1.astype(jnp.float32)
    normed = (
        hidden_wide
        * lax.rsqrt(jnp.mean(hidden_wide * hidden_wide, axis=1, keepdims=True) + epsilon)
        * ffn_gain
    ).astype(jnp.bfloat16)

    experts = n_sp * n_tp
    capacity = 4 * tokens // (n_tp * experts)
    top_count = routes.shape[1]
    width = normed.shape[1]
    slots = experts * capacity
    picks = routes.reshape(-1)
    entries = picks.shape[0]
    onehot = (picks[:, None] == jnp.arange(experts, dtype=jnp.int32)[None, :]).astype(jnp.bfloat16)
    earlier = (
        jnp.arange(entries)[None, :] < jnp.arange(entries)[:, None]
    ).astype(jnp.bfloat16)
    before = jnp.dot(earlier, onehot, preferred_element_type=jnp.float32)
    rank = jnp.sum(before * onehot.astype(jnp.float32), axis=1).astype(jnp.int32)
    place = (picks * capacity + rank).reshape(-1, top_count)
    hit = place[:, :, None] == jnp.arange(slots, dtype=jnp.int32)[None, None, :]
    share = route_weights / jnp.sum(route_weights, axis=1, keepdims=True)
    spot = jnp.any(hit, axis=1).astype(jnp.bfloat16)
    weight = jnp.sum(jnp.where(hit, share[:, :, None], 0.0), axis=1)
    high = lax.reduce_precision(weight, 8, 7)
    weights = jnp.concatenate([high, weight - high], axis=0).astype(jnp.bfloat16)

    sectioning = lax.dot_general(
        spot, normed, (((0,), (0,)), ((), ())), preferred_element_type=jnp.float32
    ).astype(jnp.bfloat16)
    received = lax.all_to_all(
        sectioning.reshape(experts, capacity, width),
        ("sp", "tp"),
        split_axis=0,
        concat_axis=0,
        tiled=True,
    )
    flat_rows = received.reshape(-1, width)
    gate_val = jnp.dot(flat_rows, gate_proj[0], preferred_element_type=jnp.float32)
    up_val = jnp.dot(flat_rows, up_proj[0], preferred_element_type=jnp.float32)
    expert_hidden = (jax.nn.silu(gate_val) * up_val).astype(jnp.bfloat16)
    done = jnp.dot(expert_hidden, down_proj[0], preferred_element_type=jnp.float32).astype(
        jnp.bfloat16
    )
    returned = lax.all_to_all(
        done.reshape(received.shape), ("sp", "tp"), split_axis=0, concat_axis=0, tiled=True
    )
    summed = jnp.dot(weights, returned.reshape(-1, width), preferred_element_type=jnp.float32)
    own = residual.shape[0]
    return (hidden_wide + (summed[:own] + summed[own:])).astype(jnp.bfloat16)


def solution(mesh):
    return jax.shard_map(
        local,
        mesh=mesh,
        in_specs=(
            P("sp", "tp"),
            P("sp", "tp"),
            P(None, None, "tp", None),
            P(None, None, "tp", None),
            P(None, None, "tp"),
            P(None, None, "tp", "sp"),
            P(None, None, "tp", None, None),
            P(None, None, "tp", None, None),
            P(None, None, "tp", None, None),
            P(None, None, "tp", None, None),
            P(None, "tp"),
            P(None, "tp", None, None),
            P(("sp", "tp"), None),
            P(),
            P(),
            P(),
            P(("sp", "tp"), None),
            P(("sp", "tp"), None),
            P(("sp", "tp"), None, None),
            P(("sp", "tp"), None, None),
            P(("sp", "tp"), None, None),
        ),
        out_specs=P(("sp", "tp"), None),
        check_vma=False,
    )
```

time: 135 us -> 108 us (0.80)
  the two profiles are of different devices: /device:TPU:9 before, /device:TPU:0 now
where the time goes in v1:
time: 108 us; the launch traced here: 107 us
  blocking collectives  32 us (30%)
  waiting for transfers between devices  26 us (24%)
  matrix products  17.4 us (16%)
  Pallas kernels  16 us (15%)
  local copies, waits for them, and re-layouts  10.9 us (10%)
  starting transfers between devices  3.62 us (3%)
  other arithmetic  1.19 us (1%)
    all_to_all x1, blocking collectives, local(): lax.all_to_all(sectioning.reshape(experts, capacity, width), ('sp', 'tp')...  32 us
    all_to_all x1, waiting for transfers between devices, local(): lax.all_to_all(done.reshape(received.shape), ('sp', 'tp'), split_axis=0,...  26 us
    pallas_call x1, Pallas kernels, mixer(): pl.pallas_call(mixer_kernel, out_shape=jax.ShapeDtypeStruct((n_tp, tokens...  16 us
    unnamed x31, local copies, waits for them, and re-layouts  10.5 us
    dot_general x1, matrix products, local(): jnp.dot(expert_hidden, down_proj[0], preferred_element_type=jnp.float32)  8.78 us
    dot_general x1, matrix products, local(): jnp.dot(flat_rows, gate_proj[0], preferred_element_type=jnp.float32)  4.43 us
    all_to_all x1, starting transfers between devices, local(): lax.all_to_all(done.reshape(received.shape), ('sp', 'tp'), split_axis=0,...  3.62 us
    dot_general x1, matrix products, local(): projected = jnp.dot(mixed, out_proj, preferred_element_type=jnp.float32)  3.25 us
  transfers between devices with their start and end apart: 1, of which 1 were waited for; matrix products, arithmetic and copies ran while one was open for 0% of the time, Pallas kernels for 0%

profile of v1, /device:TPU:0, one launch (start us, length us, event | category | flops | bytes accessed | tf_op | source)
XLA Modules:
  0.0 107.3 jit_solution(4137671420890873910)
XLA Ops:
  0.0 1.0 copy-done
  1.0 1.0 copy-done.1
  2.1 1.0 copy-done.2
  3.1 1.0 copy-done.3
  4.2 0.9 copy-done.4
  5.1 0.8 copy-done.5
  5.9 0.8 copy-done.6
  6.8 0.8 copy-done.7
  7.5 0.8 copy-done.8
  8.3 0.8 copy-done.9
  9.0 0.7 copy-done.10
  9.7 0.7 copy-done.11
  10.4 16.0 %mixer.1 = bf16[2,64,512]{2,1,0:T(8,128)(2,1)S(1)} custom-call(bf16[128,256]{1,0:T(8,128)(2,1)S(1)} %copy-done.5, bf16[128,256]{1,0:T(8,128)(2,1)S(1)} %copy-done.6, f32[2,2,16,64]{3,2,1,0:T(8,128)S(1)} %copy-done.7, f32[2,2,16,32]{3,2,1,0:T(8,128)S(1)} %copy-done.8, f32[2,2,16]{2,1,0:T(2,128)S(1)} %copy-done.10, f32[2,2,16,128]{3,2,1,0:T(8,128)S(1)} %copy-done.9, ...), custom_call_target="tpu_custom_call" | custom-call | tf_op jit(solution)/shard_map/mixer/pallas_call | solution.py:330
  26.5 0.1 fusion.33
  26.6 3.3 %multiply_reduce_fusion = (f32[64]{0:T(128)S(1)}, f32[64,2048]{1,0:T(8,128)S(1)}) fusion(bf16[1024,2048]{1,0:T(8,128)(2,1)} %param.35, f32[1024]{0:T(1024)} %param.34, f32[64]{0:T(128)S(1)} %add_rsqrt_fusion.1, bf16[64,256]{1,0:T(8,128)(2,1)S(1)} %get-tuple-element.6, bf16[64,256]{1,0:T(8,128)(2,1)S(1)} %get-tuple-element.7, ...), kind=kOutput, calls=%fused_computation.26 | convolution fusion | flops 269942720 | bytes 5116416 | tf_op jit(solution)/shard_map/dot_general | solution.py:376
  29.9 0.0 copy-done.13
  29.9 0.1 copy.34
  30.0 0.1 eq.28
  30.1 0.2 fusion.21
  30.3 0.1 convert_element_type.55
  30.4 0.1 copy.35
  30.5 0.1 fusion.39
  30.6 0.5 fusion.15
  31.1 32.0 %all_to_all.10 = bf16[32,8,2048]{2,1,0:T(8,128)(2,1)S(1)} all-to-all(bf16[32,8,2048]{2,1,0:T(8,128)(2,1)S(1)} %fusion.15), channel_id=1, replica_groups=mesh['sp'=16,'tp'=2] {'sp','tp'}, dimensions={0} | all-to-all | bytes 2097152 | tf_op jit(solution)/shard_map/all_to_all | solution.py:409
  63.1 4.4 %fusion.4 = f32[256,1408]{1,0:T(8,128)S(1)} fusion(bf16[1,2048,1408]{2,1,0:T(8,128)(2,1)} %param.39, bf16[32,8,2048]{2,1,0:T(8,128)(2,1)S(1)} %all_to_all.10), kind=kOutput, calls=%fused_computation.4 | convolution fusion | flops 1476395008 | bytes 8257536 | tf_op jit(solution)/shard_map/dot_general | solution.py:417
  67.6 0.0 copy-start.14
  67.6 8.8 %fusion.16 = bf16[32,8,2048]{2,1,0:T(8,128)(2,1)} fusion(bf16[1,1408,2048]{2,1,0:T(8,128)(2,1)} %param.41, bf16[1,2048,1408]{2,1,0:T(8,128)(2,1)} %param.40, f32[256,1408]{1,0:T(8,128)S(1)} %fusion.4, bf16[32,8,2048]{2,1,0:T(8,128)(2,1)S(1)} %all_to_all.10), kind=kOutput, calls=%fused_computation.11 | convolution fusion | flops 2955476992 | bytes 15073280 | tf_op jit(solution)/shard_map/dot_general | solution.py:420
  76.4 3.6 %all-to-all-start.1 = ((bf16[32,8,2048]{2,1,0:T(8,128)(2,1)}), bf16[32,8,2048]{2,1,0:T(8,128)(2,1)S(1)}, u32[]{:S(2)}, u32[]{:S(2)}) async-start(bf16[32,8,2048]{2,1,0:T(8,128)(2,1)} %fusion.16), calls=%async_computation.1 | async-start | bytes 2097152 | tf_op jit(solution)/shard_map/all_to_all | solution.py:423
  80.0 0.1 select_reduce_fusion
  80.2 26.0 %all-to-all-done.1 = bf16[32,8,2048]{2,1,0:T(8,128)(2,1)S(1)} async-done(((bf16[32,8,2048]{2,1,0:T(8,128)(2,1)}), bf16[32,8,2048]{2,1,0:T(8,128)(2,1)S(1)}, u32[]{:S(2)}, u32[]{:S(2)}) %all-to-all-start.1) | async-done | bytes 1048608 | tf_op jit(solution)/shard_map/all_to_all | solution.py:423
  106.2 0.3 fusion.22
  106.5 0.8 fusion.32
  (24 shorter events, 0.1 us)
Async XLA Ops:
  0.0 1.0 copy-start
  1.0 1.0 copy-start.1
  2.1 1.0 copy-start.2
  3.1 1.0 copy-start.3
  4.2 0.9 copy-start.4
  5.1 0.8 copy-start.5
  5.9 0.8 copy-start.6
  6.8 0.8 copy-start.7
  7.5 0.8 copy-start.8
  8.3 0.8 copy-start.9
  9.0 0.7 copy-start.10
  9.7 0.7 copy-start.11
  10.4 19.5 %copy-start.13 = (s32[64,2]{0,1:T(2,128)S(1)}, s32[64,2]{0,1:T(2,128)}, u32[]{:S(2)}) copy-start(s32[64,2]{0,1:T(2,128)} %param.37) | copy-start | bytes 1540
  10.4 20.2 %copy-start.12 = (f32[2048]{0:T(1024)S(1)}, f32[2048]{0:T(1024)}, u32[]{:S(2)}) copy-start(f32[2048]{0:T(1024)} %param.36) | copy-start | bytes 24580
  67.6 12.4 %copy-start.14 = (f32[64,2]{0,1:T(2,128)S(1)}, f32[64,2]{0,1:T(2,128)}, u32[]{:S(2)}) copy-start(f32[64,2]{0,1:T(2,128)} %param.38) | copy-start | bytes 1540
  76.4 29.8 %all-to-all-start.1 = ((bf16[32,8,2048]{2,1,0:T(8,128)(2,1)}), bf16[32,8,2048]{2,1,0:T(8,128)(2,1)S(1)}, u32[]{:S(2)}, u32[]{:S(2)}) async-start(bf16[32,8,2048]{2,1,0:T(8,128)(2,1)} %fusion.16), calls=%async_computation.1 | async-start | bytes 2097152 | tf_op jit(solution)/shard_map/all_to_all | solution.py:423

commit v2 on v1

--- a/solution.py
+++ b/solution.py
@@ -73,11 +73,59 @@
     return jnp.where(row == column, 1.0, 0.0).astype(jnp.bfloat16)
 
 
-def mixer_kernel(
-    wide_u, narrow_u, wide_poles, narrow_poles, step_ref, forget_ref, wide_in, narrow_in,
-    wide_out, narrow_out, skip_ref, gate_ref, out_ref,
-    signal, push, keep, ends_ref, sub_ref, all_ref, carry, mixed, send_sem, recv_sem, swap_sem,
-):
+def flip(value, bits):
+    bit = 1
+    while bit <= bits:
+        if bits & bit:
+            value = value + bit - 2 * bit * ((value // bit) % 2)
+        bit *= 2
+    return value
+
+
+def rms_scale(value, width):
+    return lax.rsqrt(jnp.sum(value * value, axis=1, keepdims=True) / width + epsilon)
+
+
+def tiles(width, tile, step):
+    full = width // tile
+    if full:
+
+        @pl.loop(0, full)
+        def _(j):
+            step(pl.ds(pl.multiple_of(j * tile, tile), tile))
+
+    if width % tile:
+        step(slice(full * tile, width))
+
+
+def chunks_of(devices):
+    near, far = min(16, devices // 2), min(16, devices // 4)
+    half = devices // 2
+    return [(a, a + near) for a in range(0, half, near)] + [
+        (a, a + far) for a in range(half, devices, far)
+    ]
+
+
+N_SMALL = 17
+
+
+def layer_kernel(*refs):
+    small_hbm, refs = refs[:N_SMALL], refs[N_SMALL:]
+    big_hbm, refs = refs[:4], refs[4:]
+    result, refs = refs[0], refs[1:]
+    small, refs = refs[:N_SMALL], refs[N_SMALL:]
+    big, refs = refs[:4], refs[4:]
+    (
+        wide_u, narrow_u, wide_poles, narrow_poles, step_ref, forget_ref, wide_in, narrow_in,
+        wide_out, narrow_out, skip_ref, gate_ref, residual, mixer_gain, ffn_gain, routes,
+        route_weights,
+    ) = small
+    gate_w, up_w, down_w, out_w = big
+    (
+        signal, push, keep, ends_ref, sub_ref, all_ref, carry, mixed, out_ref, send_r, recv_r,
+        send_m, recv_m, send_o, recv_o, own, hidden, normed, inner,
+        small_sem, big_sem, send_sem, recv_sem, swap_sem, send_sems, recv_sems,
+    ) = refs
     tokens, half = wide_u.shape
     groups, channels = wide_in.shape[2:4]
     sets = (wide_in.shape[4], narrow_in.shape[4])
@@ -89,17 +137,70 @@
     n_tp = lax.axis_size("tp")
     mine = lax.axis_index("sp")
     tp = lax.axis_index("tp")
+    devices, capacity, model = send_r.shape
+    own_rows = residual.shape[0]
+    others = [(r // n_tp, r % n_tp) for r in range(devices)]
+    peers = [{"sp": flip(mine, a), "tp": flip(tp, b)} for a, b in others]
     barrier = pltpu.get_barrier_semaphore()
-    for k in range(1, count):
+    for r in range(1, devices):
         pl.semaphore_signal(
-            barrier, inc=1, device_id={"sp": lax.rem(mine + k, count)},
-            device_id_type=pl.DeviceIdType.MESH,
-        )
-    for k in range(1, n_tp):
-        pl.semaphore_signal(
-            barrier, inc=1, device_id={"tp": lax.rem(tp + k, n_tp)},
-            device_id_type=pl.DeviceIdType.MESH,
-        )
+            barrier, inc=1, device_id=peers[r], device_id_type=pl.DeviceIdType.MESH
+        )
+    stages = []
+    for i in (15, 12, 0, 1, 5, 2, 3, 4, 6, 7, 16, 8, 9, 10, 11, 13, 14):
+        copy = pltpu.make_async_copy(small_hbm[i], small[i], small_sem.at[i])
+        copy.start()
+        stages.append(copy)
+    loads = []
+    for i in (3, 0, 1, 2):
+        source = big_hbm[i] if i == 3 else big_hbm[i].at[0]
+        copy = pltpu.make_async_copy(source, big[i], big_sem.at[i])
+        copy.start()
+        loads.append(copy)
+
+    def exchange(which, source, target, r):
+        return pltpu.make_async_remote_copy(
+            src_ref=source.at[r], dst_ref=target.at[r],
+            send_sem=send_sems.at[which, r], recv_sem=recv_sems.at[which, r],
+            device_id=peers[r], device_id_type=pl.DeviceIdType.MESH,
+        )
+
+    for copy in stages[:2]:
+        copy.wait()
+    slots = devices * capacity
+    slot = lax.broadcasted_iota(jnp.int32, (own_rows, slots), 1)
+    expert = (slot // capacity) ^ (mine * n_tp + tp)
+    picked = [routes[:, k : k + 1] == expert for k in range(routes.shape[1])]
+    chosen = picked[0]
+    for each in picked[1:]:
+        chosen = jnp.logical_or(chosen, each)
+    chosen = jnp.where(chosen, 1.0, 0.0)
+    earlier = jnp.where(
+        lax.broadcasted_iota(jnp.int32, (own_rows, own_rows), 0)
+        > lax.broadcasted_iota(jnp.int32, (own_rows, own_rows), 1),
+        1.0, 0.0,
+    ).astype(jnp.bfloat16)
+    rank = jnp.dot(earlier, chosen.astype(jnp.bfloat16), preferred_element_type=jnp.float32)
+    here = rank == (slot % capacity).astype(jnp.float32)
+    spot = jnp.where(here, chosen, 0.0).T.astype(jnp.bfloat16)
+
+    def sections(value):
+        rows = jnp.dot(spot, value, preferred_element_type=jnp.float32)
+        return rows.reshape(devices, capacity, value.shape[1]).astype(jnp.bfloat16)
+
+    tile = min(512, model)
+    for a in range(0, model, tile):
+        send_r[:, :, a : a + tile] = sections(residual[:, a : a + tile])
+    recv_r[0] = send_r[0]
+    pl.semaphore_wait(barrier, devices - 1)
+    far = list(range(devices // 2, devices))
+    near = list(range(1, devices // 2))
+    first = min(4, len(far))
+    early = [exchange(0, send_r, recv_r, r) for r in far[:first]]
+    for copy in early:
+        copy.start()
+    for copy in stages[2:]:
+        copy.wait()
 
     row = lax.broadcasted_iota(jnp.int32, (tokens, tokens), 0)
     column = lax.broadcasted_iota(jnp.int32, (tokens, tokens), 1)
@@ -205,7 +306,7 @@
             put(direction, 0, column, e_re)
             put(direction, 1, column, e_im)
 
-    pl.semaphore_wait(barrier, count - 1 + n_tp - 1)
+
     copies = []
     for k in range(1, count):
         copy = pltpu.make_async_remote_copy(
@@ -219,6 +320,10 @@
         copy.start()
         copies.append(copy)
     all_ref[mine] = jnp.zeros(ends_ref.shape[1:], jnp.float32)
+
+    late = [exchange(0, send_r, recv_r, r) for r in far[first:] + near]
+    for copy in late:
+        copy.start()
     for copy in copies:
         copy.wait()
 
@@ -319,113 +424,165 @@
         copy.wait()
 
 
-def mixer(*args):
-    tokens, half = args[0].shape
-    groups, channels, wide_state = args[6].shape[2:]
-    narrow_state = args[7].shape[4]
+    parts = [
+        (out_ref[k, :, which * half : (which + 1) * half], which, k)
+        for which in range(2) for k in range(n_tp)
+    ]
+    joined = jnp.concatenate([value.astype(jnp.float32) for value, _, _ in parts], axis=1)
+    scale = rms_scale(joined, joined.shape[1])
+    moved = (joined * scale * mixer_gain[...]).astype(jnp.bfloat16)
+    send_m[...] = sections(moved)
+    recv_m[0] = send_m[0]
+    order_m = far + near
+    outs = [exchange(1, send_m, recv_m, r) for r in order_m]
+    for copy in outs:
+        copy.start()
+    share = route_weights[...]
+    total_share = share[:, 0:1]
+    for k in range(1, share.shape[1]):
+        total_share = total_share + share[:, k : k + 1]
+    weight = jnp.zeros((own_rows, slots), jnp.float32)
+    for k, each in enumerate(picked):
+        weight = weight + jnp.where(
+            jnp.logical_and(each, here), share[:, k : k + 1] / total_share, 0.0
+        )
+    high = weight.astype(jnp.bfloat16)
+    weights = jnp.concatenate([high, (weight - high.astype(jnp.float32)).astype(jnp.bfloat16)], axis=0)
+    loads[0].wait()
+
+    def own_hidden(cols):
+        value = residual[:, cols].astype(jnp.float32) + jnp.dot(
+            moved, out_w[:, cols], preferred_element_type=jnp.float32
+        )
+        own[:, cols] = value.astype(jnp.bfloat16).astype(jnp.float32)
+
+    tiles(model, 512, own_hidden)
+    for copy in loads[1:]:
+        copy.wait()
+    backs = []
+    for a, b in chunks_of(devices):
+        for r in range(max(a, 1), b):
+            exchange(0, send_r, recv_r, r).wait_recv()
+            exchange(1, send_m, recv_m, r).wait_recv()
+        rows = (b - a) * capacity
+        arrived = recv_m[a:b].astype(jnp.float32).reshape(rows, -1).astype(jnp.bfloat16)
+
+        def full_hidden(cols, a=a, b=b, rows=rows, arrived=arrived):
+            value = recv_r[a:b, :, cols].astype(jnp.float32).reshape(rows, -1) + jnp.dot(
+                arrived, out_w[:, cols], preferred_element_type=jnp.float32
+            )
+            hidden[:rows, cols] = value.astype(jnp.bfloat16).astype(jnp.float32)
+
+        tiles(model, 512, full_hidden)
+        value = hidden[:rows, :]
+        normed[:rows, :] = (value * rms_scale(value, model) * ffn_gain[...]).astype(jnp.bfloat16)
+
+        def up(cols, rows=rows):
+            value = normed[:rows, :]
+            gate_val = jnp.dot(value, gate_w[:, cols], preferred_element_type=jnp.float32)
+            up_val = jnp.dot(value, up_w[:, cols], preferred_element_type=jnp.float32)
+            inner[:rows, cols] = (jax.nn.silu(gate_val) * up_val).astype(jnp.bfloat16)
+
+        tiles(inner.shape[1], 256, up)
+
+        def down(cols, a=a, b=b, rows=rows):
+            value = jnp.dot(inner[:rows, :], down_w[:, cols], preferred_element_type=jnp.float32)
+            send_o[a:b, :, cols] = value.reshape(b - a, capacity, -1).astype(jnp.bfloat16)
+
+        tiles(model, 512, down)
+        if a == 0:
+            recv_o[0] = send_o[0]
+        for r in range(max(a, 1), b):
+            copy = exchange(2, send_o, recv_o, r)
+            copy.start()
+            backs.append(copy)
+    for a, b in chunks_of(devices):
+        for r in range(max(a, 1), b):
+            exchange(2, send_o, recv_o, r).wait_recv()
+        cut = weights[:, a * capacity : b * capacity]
+
+        def gather(cols, a=a, b=b, cut=cut):
+            rows = recv_o[a:b, :, cols].astype(jnp.float32)
+            rows = rows.reshape((b - a) * capacity, -1).astype(jnp.bfloat16)
+            both = jnp.dot(cut, rows, preferred_element_type=jnp.float32)
+            own[:, cols] = own[:, cols] + (both[:own_rows] + both[own_rows:])
+
+        tiles(model, 512, gather)
+    result[...] = own[...].astype(jnp.bfloat16)
+    for copy in early + late + outs + backs:
+        copy.wait_send()
+
+
+def local(*args):
+    args = list(args)
+    names = (
+        "wide_inputs", "narrow_inputs", "wide_poles", "narrow_poles", "step_sizes", "forget",
+        "wide_in_map", "narrow_in_map", "wide_out_map", "narrow_out_map", "skip_weight",
+        "gate_mix", "residual", "mixer_gain", "out_proj", "ffn_gain", "routes", "route_weights",
+        "gate_proj", "up_proj", "down_proj",
+    )
+    by = dict(zip(names, args))
+    by["mixer_gain"] = by["mixer_gain"].reshape(1, -1)
+    by["ffn_gain"] = by["ffn_gain"].reshape(1, -1)
+    small = [by[n] for n in names if n not in ("gate_proj", "up_proj", "down_proj", "out_proj") and n not in ("mixer_gain", "ffn_gain", "routes", "route_weights")]
+    small += [by[n] for n in ("mixer_gain", "ffn_gain", "routes", "route_weights")]
+    big = [by[n] for n in ("gate_proj", "up_proj", "down_proj", "out_proj")]
+    tokens, half = by["wide_inputs"].shape
+    groups, channels, wide_state = by["wide_in_map"].shape[2:]
+    narrow_state = by["narrow_in_map"].shape[4]
     _, total = pack_list(channels, groups, (wide_state, narrow_state))
     count, n_tp = lax.axis_size("sp"), lax.axis_size("tp")
+    devices = count * n_tp
+    own_rows, width = by["residual"].shape
+    hidden_width = by["gate_proj"].shape[2]
+    capacity = max(4 * tokens // (n_tp * devices), SUBLANES)
+    joined = 2 * half * n_tp
     span = total // 3
+    chunk = max(b - a for a, b in chunks_of(devices)) * capacity
     vmem = pl.BlockSpec(memory_space=pltpu.VMEM)
+    hbm = pl.BlockSpec(memory_space=pltpu.HBM)
+    f32, bf16 = jnp.float32, jnp.bfloat16
+    dma = pltpu.SemaphoreType.DMA
     return pl.pallas_call(
-        mixer_kernel,
-        out_shape=jax.ShapeDtypeStruct((n_tp, tokens // n_tp, 2 * half), jnp.bfloat16),
-        in_specs=[vmem] * len(args),
+        layer_kernel,
+        out_shape=jax.ShapeDtypeStruct((own_rows, width), bf16),
+        in_specs=[hbm] * (len(small) + len(big)),
         out_specs=vmem,
-        scratch_shapes=[
-            pltpu.VMEM((tokens, 2 * half), jnp.bfloat16),
-            pltpu.VMEM((2, 2, tokens, total), jnp.float32),
-            pltpu.VMEM((2, tokens, total), jnp.float32),
-            pltpu.VMEM((2, 8, span), jnp.float32),
-            pltpu.VMEM((2, 4, SUBLANES, total), jnp.float32),
-            pltpu.VMEM((count, 8, span), jnp.float32),
-            pltpu.VMEM((2, 2, SUBLANES, total), jnp.float32),
-            pltpu.VMEM((tokens, 2 * half), jnp.bfloat16),
-            pltpu.SemaphoreType.DMA((count,)),
-            pltpu.SemaphoreType.DMA((count,)),
-            pltpu.SemaphoreType.DMA((2, n_tp)),
+        scratch_shapes=[pltpu.VMEM(x.shape, x.dtype) for x in small]
+        + [pltpu.VMEM(x.shape[-2:], x.dtype) for x in big]
+        + [
+            pltpu.VMEM((tokens, 2 * half), bf16),
+            pltpu.VMEM((2, 2, tokens, total), f32),
+            pltpu.VMEM((2, tokens, total), f32),
+            pltpu.VMEM((2, 8, span), f32),
+            pltpu.VMEM((2, 4, SUBLANES, total), f32),
+            pltpu.VMEM((count, 8, span), f32),
+            pltpu.VMEM((2, 2, SUBLANES, total), f32),
+            pltpu.VMEM((tokens, 2 * half), bf16),
+            pltpu.VMEM((n_tp, own_rows, 2 * half), bf16),
+            pltpu.VMEM((devices, capacity, width), bf16),
+            pltpu.VMEM((devices, capacity, width), bf16),
+            pltpu.VMEM((devices, capacity, joined), bf16),
+            pltpu.VMEM((devices, capacity, joined), bf16),
+            pltpu.VMEM((devices, capacity, width), bf16),
+            pltpu.VMEM((devices, capacity, width), bf16),
+            pltpu.VMEM((own_rows, width), f32),
+            pltpu.VMEM((chunk, width), f32),
+            pltpu.VMEM((chunk, width), bf16),
+            pltpu.VMEM((chunk, hidden_width), bf16),
+            dma((len(small),)),
+            dma((4,)),
+            dma((count,)),
+            dma((count,)),
+            dma((2, n_tp)),
+            dma((3, devices)),
+            dma((3, devices)),
         ],
         compiler_params=pltpu.CompilerParams(
-            collective_id=0, has_side_effects=True, vmem_limit_bytes=24 << 20
+            collective_id=0, has_side_effects=True, vmem_limit_bytes=60 << 20
         ),
-        name="mixer",
-    )(*args)
-
-
-def local(
-    wide_inputs, narrow_inputs, wide_poles, narrow_poles, step_sizes, forget, wide_in_map,
-    narrow_in_map, wide_out_map, narrow_out_map, skip_weight, gate_mix, residual, mixer_gain,
-    out_proj, ffn_gain, routes, route_weights, gate_proj, up_proj, down_proj,
-):
-    n_sp = lax.axis_size("sp")
-    n_tp = lax.axis_size("tp")
-    set_out = mixer(
-        wide_inputs, narrow_inputs, wide_poles, narrow_poles, step_sizes, forget, wide_in_map,
-        narrow_in_map, wide_out_map, narrow_out_map, skip_weight, gate_mix,
-    )
-    swapped = set_out
-    rows = swapped.shape[1]
-    tokens = rows * n_tp
-    half = set_out.shape[2] // 2
-    joined = jnp.concatenate(
-        [swapped[k, :, :half] for k in range(n_tp)] + [swapped[k, :, half:] for k in range(n_tp)],
-        axis=1,
-    ).astype(jnp.float32)
-    scale = lax.rsqrt(jnp.mean(joined * joined, axis=1, keepdims=True) + epsilon)
-    mixed = (joined * scale * mixer_gain).astype(jnp.bfloat16)
-    projected = jnp.dot(mixed, out_proj, preferred_element_type=jnp.float32)
-    hidden1 = (residual.astype(jnp.float32) + projected).astype(jnp.bfloat16)
-    hidden_wide = hidden1.astype(jnp.float32)
-    normed = (
-        hidden_wide
-        * lax.rsqrt(jnp.mean(hidden_wide * hidden_wide, axis=1, keepdims=True) + epsilon)
-        * ffn_gain
-    ).astype(jnp.bfloat16)
-
-    experts = n_sp * n_tp
-    capacity = 4 * tokens // (n_tp * experts)
-    top_count = routes.shape[1]
-    width = normed.shape[1]
-    slots = experts * capacity
-    picks = routes.reshape(-1)
-    entries = picks.shape[0]
-    onehot = (picks[:, None] == jnp.arange(experts, dtype=jnp.int32)[None, :]).astype(jnp.bfloat16)
-    earlier = (
-        jnp.arange(entries)[None, :] < jnp.arange(entries)[:, None]
-    ).astype(jnp.bfloat16)
-    before = jnp.dot(earlier, onehot, preferred_element_type=jnp.float32)
-    rank = jnp.sum(before * onehot.astype(jnp.float32), axis=1).astype(jnp.int32)
-    place = (picks * capacity + rank).reshape(-1, top_count)
-    hit = place[:, :, None] == jnp.arange(slots, dtype=jnp.int32)[None, None, :]
-    share = route_weights / jnp.sum(route_weights, axis=1, keepdims=True)
-    spot = jnp.any(hit, axis=1).astype(jnp.bfloat16)
-    weight = jnp.sum(jnp.where(hit, share[:, :, None], 0.0), axis=1)
-    high = lax.reduce_precision(weight, 8, 7)
-    weights = jnp.concatenate([high, weight - high], axis=0).astype(jnp.bfloat16)
-
-    sectioning = lax.dot_general(
-        spot, normed, (((0,), (0,)), ((), ())), preferred_element_type=jnp.float32
-    ).astype(jnp.bfloat16)
-    received = lax.all_to_all(
-        sectioning.reshape(experts, capacity, width),
-        ("sp", "tp"),
-        split_axis=0,
-        concat_axis=0,
-        tiled=True,
-    )
-    flat_rows = received.reshape(-1, width)
-    gate_val = jnp.dot(flat_rows, gate_proj[0], preferred_element_type=jnp.float32)
-    up_val = jnp.dot(flat_rows, up_proj[0], preferred_element_type=jnp.float32)
-    expert_hidden = (jax.nn.silu(gate_val) * up_val).astype(jnp.bfloat16)
-    done = jnp.dot(expert_hidden, down_proj[0], preferred_element_type=jnp.float32).astype(
-        jnp.bfloat16
-    )
-    returned = lax.all_to_all(
-        done.reshape(received.shape), ("sp", "tp"), split_axis=0, concat_axis=0, tiled=True
-    )
-    summed = jnp.dot(weights, returned.reshape(-1, width), preferred_element_type=jnp.float32)
-    own = residual.shape[0]
-    return (hidden_wide + (summed[:own] + summed[own:])).astype(jnp.bfloat16)
+        name="layer",
+    )(*small, *big)
 
 
 def solution(mesh):

time: 108 us -> 84.9 us (0.79)
  the two profiles are of different devices: /device:TPU:0 before, /device:TPU:9 now
where the time goes in v2:
time: 84.9 us; the launch traced here: 84.8 us
  Pallas kernels  80.3 us (95%)
  local copies, waits for them, and re-layouts  4.42 us (5%)
    pallas_call x1, Pallas kernels, local(): pl.pallas_call(layer_kernel, out_shape=jax.ShapeDtypeStruct((own_rows, wi...  80.3 us
    unnamed x3, local copies, waits for them, and re-layouts  4.42 us

profile of v2, /device:TPU:9, one launch (start us, length us, event | category | flops | bytes accessed | tf_op | source)
XLA Modules:
  0.0 84.8 jit_solution(12753686955073586829)
XLA Ops:
  0.0 1.4 %copy.22.refs_15_ = s32[64,2]{1,0:T(8,128)} copy(s32[64,2]{0,1:T(2,128)} %param.37) | data formatting | bytes 1024 | tf_op args[16]
  1.4 1.4 %copy.23.refs_16_ = f32[64,2]{1,0:T(8,128)} copy(f32[64,2]{0,1:T(2,128)} %param.38) | data formatting | bytes 1024 | tf_op args[17]
  2.7 80.3 %layer.1 = bf16[64,2048]{1,0:T(8,128)(2,1)} custom-call(bf16[128,256]{1,0:T(8,128)(2,1)} %refs_0_.1, bf16[128,256]{1,0:T(8,128)(2,1)} %refs_1_.1, f32[2,2,16,64]{3,2,1,0:T(8,128)} %refs_2_.1, f32[2,2,16,32]{3,2,1,0:T(8,128)} %refs_3_.1, f32[2,2,16]{2,1,0:T(2,128)} %refs_4_.1, f32[2,2,16,128]{3,2,1,0:T(8,128)} %refs_5_.1, f32[2,2,16,16,64]{4,3,2,1,0:T(8,128)} %refs_6_.1, ...), custom_call_target="tpu_custom_call" | custom-call | tf_op jit(solution)/shard_map/layer/pallas_call | solution.py:546
  83.1 1.7 %copy.25 = bf16[64,2048]{1,0:T(8,128)(2,1)} copy(bf16[64,2048]{1,0:T(8,128)(2,1)} %layer.1) | data formatting | bytes 524288

commit v3 on v2

--- a/solution.py
+++ b/solution.py
@@ -104,6 +104,13 @@
     return [(a, a + near) for a in range(0, half, near)] + [
         (a, a + far) for a in range(half, devices, far)
     ]
+
+
+def send_order(devices):
+    half, quarter = devices // 2, devices // 4
+    first = list(range(half, half + quarter))
+    near = list(range(1, half))
+    return first + near + list(range(half + quarter, devices))
 
 
 N_SMALL = 17
@@ -122,8 +129,8 @@
     ) = small
     gate_w, up_w, down_w, out_w = big
     (
-        signal, push, keep, ends_ref, sub_ref, all_ref, carry, mixed, out_ref, send_r, recv_r,
-        send_m, recv_m, send_o, recv_o, own, hidden, normed, inner,
+        signal, push, keep, ends_ref, sub_ref, all_ref, carry, mixed, out_ref, send_d, recv_d,
+        send_o, recv_o, own, normed, inner,
         small_sem, big_sem, send_sem, recv_sem, swap_sem, send_sems, recv_sems,
     ) = refs
     tokens, half = wide_u.shape
@@ -137,7 +144,7 @@
     n_tp = lax.axis_size("tp")
     mine = lax.axis_index("sp")
     tp = lax.axis_index("tp")
-    devices, capacity, model = send_r.shape
+    devices, capacity, model = send_d.shape
     own_rows = residual.shape[0]
     others = [(r // n_tp, r % n_tp) for r in range(devices)]
     peers = [{"sp": flip(mine, a), "tp": flip(tp, b)} for a, b in others]
@@ -147,16 +154,14 @@
             barrier, inc=1, device_id=peers[r], device_id_type=pl.DeviceIdType.MESH
         )
     stages = []
-    for i in (15, 12, 0, 1, 5, 2, 3, 4, 6, 7, 16, 8, 9, 10, 11, 13, 14):
+    for i in (0, 1, 5, 2, 3, 4, 6, 7, 8, 9, 10, 11, 12, 13, 14, 15, 16):
         copy = pltpu.make_async_copy(small_hbm[i], small[i], small_sem.at[i])
         copy.start()
         stages.append(copy)
     loads = []
     for i in (3, 0, 1, 2):
         source = big_hbm[i] if i == 3 else big_hbm[i].at[0]
-        copy = pltpu.make_async_copy(source, big[i], big_sem.at[i])
-        copy.start()
-        loads.append(copy)
+        loads.append(pltpu.make_async_copy(source, big[i], big_sem.at[i]))
 
     def exchange(which, source, target, r):
         return pltpu.make_async_remote_copy(
@@ -165,42 +170,10 @@
             device_id=peers[r], device_id_type=pl.DeviceIdType.MESH,
         )
 
-    for copy in stages[:2]:
+    for copy in stages:
         copy.wait()
-    slots = devices * capacity
-    slot = lax.broadcasted_iota(jnp.int32, (own_rows, slots), 1)
-    expert = (slot // capacity) ^ (mine * n_tp + tp)
-    picked = [routes[:, k : k + 1] == expert for k in range(routes.shape[1])]
-    chosen = picked[0]
-    for each in picked[1:]:
-        chosen = jnp.logical_or(chosen, each)
-    chosen = jnp.where(chosen, 1.0, 0.0)
-    earlier = jnp.where(
-        lax.broadcasted_iota(jnp.int32, (own_rows, own_rows), 0)
-        > lax.broadcasted_iota(jnp.int32, (own_rows, own_rows), 1),
-        1.0, 0.0,
-    ).astype(jnp.bfloat16)
-    rank = jnp.dot(earlier, chosen.astype(jnp.bfloat16), preferred_element_type=jnp.float32)
-    here = rank == (slot % capacity).astype(jnp.float32)
-    spot = jnp.where(here, chosen, 0.0).T.astype(jnp.bfloat16)
-
-    def sections(value):
-        rows = jnp.dot(spot, value, preferred_element_type=jnp.float32)
-        return rows.reshape(devices, capacity, value.shape[1]).astype(jnp.bfloat16)
-
-    tile = min(512, model)
-    for a in range(0, model, tile):
-        send_r[:, :, a : a + tile] = sections(residual[:, a : a + tile])
-    recv_r[0] = send_r[0]
-    pl.semaphore_wait(barrier, devices - 1)
-    far = list(range(devices // 2, devices))
-    near = list(range(1, devices // 2))
-    first = min(4, len(far))
-    early = [exchange(0, send_r, recv_r, r) for r in far[:first]]
-    for copy in early:
+    for copy in loads:
         copy.start()
-    for copy in stages[2:]:
-        copy.wait()
 
     row = lax.broadcasted_iota(jnp.int32, (tokens, tokens), 0)
     column = lax.broadcasted_iota(jnp.int32, (tokens, tokens), 1)
@@ -307,6 +280,7 @@
             put(direction, 1, column, e_im)
 
 
+    pl.semaphore_wait(barrier, devices - 1)
     copies = []
     for k in range(1, count):
         copy = pltpu.make_async_remote_copy(
@@ -321,9 +295,36 @@
         copies.append(copy)
     all_ref[mine] = jnp.zeros(ends_ref.shape[1:], jnp.float32)
 
-    late = [exchange(0, send_r, recv_r, r) for r in far[first:] + near]
-    for copy in late:
-        copy.start()
+    slots = devices * capacity
+    slot = lax.broadcasted_iota(jnp.int32, (slots, own_rows), 0)
+    expert = (slot // capacity) ^ (mine * n_tp + tp)
+    picked = [routes[k : k + 1, :] == expert for k in range(routes.shape[0])]
+    chosen = picked[0]
+    for each in picked[1:]:
+        chosen = jnp.logical_or(chosen, each)
+    chosen = jnp.where(chosen, 1.0, 0.0)
+    earlier = jnp.where(
+        lax.broadcasted_iota(jnp.int32, (own_rows, own_rows), 0)
+        < lax.broadcasted_iota(jnp.int32, (own_rows, own_rows), 1),
+        1.0, 0.0,
+    ).astype(jnp.bfloat16)
+    rank = jnp.dot(chosen.astype(jnp.bfloat16), earlier, preferred_element_type=jnp.float32)
+    here = rank == (slot % capacity).astype(jnp.float32)
+    spot = jnp.where(here, chosen, 0.0).astype(jnp.bfloat16)
+    share = route_weights[...]
+    total_share = share[0:1]
+    for k in range(1, share.shape[0]):
+        total_share = total_share + share[k : k + 1]
+    weight = jnp.zeros((slots, own_rows), jnp.float32)
+    for k, each in enumerate(picked):
+        weight = weight + jnp.where(
+            jnp.logical_and(each, here), share[k : k + 1] / total_share, 0.0
+        )
+    weight = weight.T
+    high = weight.astype(jnp.bfloat16)
+    weights = jnp.concatenate(
+        [high, (weight - high.astype(jnp.float32)).astype(jnp.bfloat16)], axis=0
+    )
     for copy in copies:
         copy.wait()
 
@@ -431,23 +432,6 @@
     joined = jnp.concatenate([value.astype(jnp.float32) for value, _, _ in parts], axis=1)
     scale = rms_scale(joined, joined.shape[1])
     moved = (joined * scale * mixer_gain[...]).astype(jnp.bfloat16)
-    send_m[...] = sections(moved)
-    recv_m[0] = send_m[0]
-    order_m = far + near
-    outs = [exchange(1, send_m, recv_m, r) for r in order_m]
-    for copy in outs:
-        copy.start()
-    share = route_weights[...]
-    total_share = share[:, 0:1]
-    for k in range(1, share.shape[1]):
-        total_share = total_share + share[:, k : k + 1]
-    weight = jnp.zeros((own_rows, slots), jnp.float32)
-    for k, each in enumerate(picked):
-        weight = weight + jnp.where(
-            jnp.logical_and(each, here), share[:, k : k + 1] / total_share, 0.0
-        )
-    high = weight.astype(jnp.bfloat16)
-    weights = jnp.concatenate([high, (weight - high.astype(jnp.float32)).astype(jnp.bfloat16)], axis=0)
     loads[0].wait()
 
     def own_hidden(cols):
@@ -457,25 +441,31 @@
         own[:, cols] = value.astype(jnp.bfloat16).astype(jnp.float32)
 
     tiles(model, 512, own_hidden)
+    scale = rms_scale(own[...], model)
+
+    def dispatch(cols):
+        value = (own[:, cols] * scale * ffn_gain[:, cols]).astype(jnp.bfloat16)
+        rows = jnp.dot(spot, value, preferred_element_type=jnp.float32)
+        send_d[:, :, cols] = rows.reshape(devices, capacity, -1).astype(jnp.bfloat16)
+
+    tiles(model, 512, dispatch)
+    recv_d[0] = send_d[0]
+    outs = [exchange(0, send_d, recv_d, r) for r in send_order(devices)]
+    for copy in outs:
+        copy.start()
     for copy in loads[1:]:
         copy.wait()
     backs = []
     for a, b in chunks_of(devices):
         for r in range(max(a, 1), b):
-            exchange(0, send_r, recv_r, r).wait_recv()
-            exchange(1, send_m, recv_m, r).wait_recv()
+            exchange(0, send_d, recv_d, r).wait_recv()
         rows = (b - a) * capacity
-        arrived = recv_m[a:b].astype(jnp.float32).reshape(rows, -1).astype(jnp.bfloat16)
-
-        def full_hidden(cols, a=a, b=b, rows=rows, arrived=arrived):
-            value = recv_r[a:b, :, cols].astype(jnp.float32).reshape(rows, -1) + jnp.dot(
-                arrived, out_w[:, cols], preferred_element_type=jnp.float32
-            )
-            hidden[:rows, cols] = value.astype(jnp.bfloat16).astype(jnp.float32)
-
-        tiles(model, 512, full_hidden)
-        value = hidden[:rows, :]
-        normed[:rows, :] = (value * rms_scale(value, model) * ffn_gain[...]).astype(jnp.bfloat16)
+
+        def arrange(cols, a=a, b=b, rows=rows):
+            value = recv_d[a:b, :, cols].astype(jnp.float32).reshape(rows, -1)
+            normed[:rows, cols] = value.astype(jnp.bfloat16)
+
+        tiles(model, 512, arrange)
 
         def up(cols, rows=rows):
             value = normed[:rows, :]
@@ -493,23 +483,23 @@
         if a == 0:
             recv_o[0] = send_o[0]
         for r in range(max(a, 1), b):
-            copy = exchange(2, send_o, recv_o, r)
+            copy = exchange(1, send_o, recv_o, r)
             copy.start()
             backs.append(copy)
     for a, b in chunks_of(devices):
         for r in range(max(a, 1), b):
-            exchange(2, send_o, recv_o, r).wait_recv()
-        cut = weights[:, a * capacity : b * capacity]
-
-        def gather(cols, a=a, b=b, cut=cut):
+            exchange(1, send_o, recv_o, r).wait_recv()
+        part = weights[:, a * capacity : b * capacity]
+
+        def gather(cols, a=a, b=b, part=part):
             rows = recv_o[a:b, :, cols].astype(jnp.float32)
             rows = rows.reshape((b - a) * capacity, -1).astype(jnp.bfloat16)
-            both = jnp.dot(cut, rows, preferred_element_type=jnp.float32)
+            both = jnp.dot(part, rows, preferred_element_type=jnp.float32)
             own[:, cols] = own[:, cols] + (both[:own_rows] + both[own_rows:])
 
         tiles(model, 512, gather)
     result[...] = own[...].astype(jnp.bfloat16)
-    for copy in early + late + outs + backs:
+    for copy in outs + backs:
         copy.wait_send()
 
 
@@ -524,6 +514,8 @@
     by = dict(zip(names, args))
     by["mixer_gain"] = by["mixer_gain"].reshape(1, -1)
     by["ffn_gain"] = by["ffn_gain"].reshape(1, -1)
+    by["routes"] = by["routes"].T
+    by["route_weights"] = by["route_weights"].T
     small = [by[n] for n in names if n not in ("gate_proj", "up_proj", "down_proj", "out_proj") and n not in ("mixer_gain", "ffn_gain", "routes", "route_weights")]
     small += [by[n] for n in ("mixer_gain", "ffn_gain", "routes", "route_weights")]
     big = [by[n] for n in ("gate_proj", "up_proj", "down_proj", "out_proj")]
@@ -536,7 +528,6 @@
     own_rows, width = by["residual"].shape
     hidden_width = by["gate_proj"].shape[2]
     capacity = max(4 * tokens // (n_tp * devices), SUBLANES)
-    joined = 2 * half * n_tp
     span = total // 3
     chunk = max(b - a for a, b in chunks_of(devices)) * capacity
     vmem = pl.BlockSpec(memory_space=pltpu.VMEM)
@@ -562,12 +553,9 @@
             pltpu.VMEM((n_tp, own_rows, 2 * half), bf16),
             pltpu.VMEM((devices, capacity, width), bf16),
             pltpu.VMEM((devices, capacity, width), bf16),
-            pltpu.VMEM((devices, capacity, joined), bf16),
-            pltpu.VMEM((devices, capacity, joined), bf16),
             pltpu.VMEM((devices, capacity, width), bf16),
             pltpu.VMEM((devices, capacity, width), bf16),
             pltpu.VMEM((own_rows, width), f32),
-            pltpu.VMEM((chunk, width), f32),
             pltpu.VMEM((chunk, width), bf16),
             pltpu.VMEM((chunk, hidden_width), bf16),
             dma((len(small),)),
@@ -575,8 +563,8 @@
             dma((count,)),
             dma((count,)),
             dma((2, n_tp)),
-            dma((3, devices)),
-            dma((3, devices)),
+            dma((2, devices)),
+            dma((2, devices)),
         ],
         compiler_params=pltpu.CompilerParams(
             collective_id=0, has_side_effects=True, vmem_limit_bytes=60 << 20

time: 84.9 us -> 73.4 us (0.86)
  Pallas kernels: 80.3 us -> 71.5 us
  local copies, waits for them, and re-layouts: 4.42 us -> 1.67 us
    pallas_call x1, Pallas kernels: 80.3 us -> 71.5 us  [local(): pl.pallas_call(layer_kernel, out_shape=jax.ShapeDtypeStruct((own_rows, wi...]
    unnamed x3 -> x1, local copies, waits for them, and re-layouts: 4.42 us -> 1.67 us
where the time goes in v3:
time: 73.4 us; the launch traced here: 73.2 us
  Pallas kernels  71.5 us (97%)
  local copies, waits for them, and re-layouts  1.67 us (2%)
    pallas_call x1, Pallas kernels, local(): pl.pallas_call(layer_kernel, out_shape=jax.ShapeDtypeStruct((own_rows, wi...  71.5 us
    unnamed x1, local copies, waits for them, and re-layouts  1.67 us

profile of v3, /device:TPU:9, one launch (start us, length us, event | category | flops | bytes accessed | tf_op | source)
XLA Modules:
  0.0 73.2 jit_solution(17939759314058895598)
XLA Ops:
  0.0 71.5 %layer.1 = bf16[64,2048]{1,0:T(8,128)(2,1)} custom-call(bf16[128,256]{1,0:T(8,128)(2,1)} %refs_0_.1, bf16[128,256]{1,0:T(8,128)(2,1)} %refs_1_.1, f32[2,2,16,64]{3,2,1,0:T(8,128)} %refs_2_.1, f32[2,2,16,32]{3,2,1,0:T(8,128)} %refs_3_.1, f32[2,2,16]{2,1,0:T(2,128)} %refs_4_.1, f32[2,2,16,128]{3,2,1,0:T(8,128)} %refs_5_.1, f32[2,2,16,16,64]{4,3,2,1,0:T(8,128)} %refs_6_.1, ...), custom_call_target="tpu_custom_call" | custom-call | tf_op jit(solution)/shard_map/layer/pallas_call | solution.py:537
  71.5 1.7 %copy.23 = bf16[64,2048]{1,0:T(8,128)(2,1)} copy(bf16[64,2048]{1,0:T(8,128)(2,1)} %layer.1) | data formatting | bytes 524288

commit v4 on v3

--- a/solution.py
+++ b/solution.py
@@ -8,6 +8,7 @@
 epsilon = 1e-06
 SUBLANES = 8
 LANES = 128
+TILE = 512
 
 
 def complex_power(re, im, exponent):
@@ -110,7 +111,7 @@
     half, quarter = devices // 2, devices // 4
     first = list(range(half, half + quarter))
     near = list(range(1, half))
-    return first + near + list(range(half + quarter, devices))
+    return first, near + list(range(half + quarter, devices))
 
 
 N_SMALL = 17
@@ -129,7 +130,7 @@
     ) = small
     gate_w, up_w, down_w, out_w = big
     (
-        signal, push, keep, ends_ref, sub_ref, all_ref, carry, mixed, out_ref, send_d, recv_d,
+        signal, push, keep, ends_ref, ends_wide, sub_ref, all_ref, all_wide, carry, leave, gates, mixed, out_ref, send_d, recv_d,
         send_o, recv_o, own, normed, inner,
         small_sem, big_sem, send_sem, recv_sem, swap_sem, send_sems, recv_sems,
     ) = refs
@@ -163,14 +164,28 @@
         source = big_hbm[i] if i == 3 else big_hbm[i].at[0]
         loads.append(pltpu.make_async_copy(source, big[i], big_sem.at[i]))
 
-    def exchange(which, source, target, r):
+    spans = chunks_of(devices)
+
+    def group_of(r):
+        return [a <= r < b for a, b in spans].index(True)
+
+    def whole(which, source, target, first, last):
+        at = pl.ds(first, last - first)
         return pltpu.make_async_remote_copy(
-            src_ref=source.at[r], dst_ref=target.at[r],
-            send_sem=send_sems.at[which, r], recv_sem=recv_sems.at[which, r],
+            src_ref=source.at[at], dst_ref=target.at[at],
+            send_sem=send_sems.at[which], recv_sem=recv_sems.at[which, group_of(first)],
+            device_id=peers[1], device_id_type=pl.DeviceIdType.MESH,
+        )
+
+    def exchange(which, source, target, r, part=None):
+        at = (r,) if part is None else (r, slice(None), slice(part * TILE, (part + 1) * TILE))
+        return pltpu.make_async_remote_copy(
+            src_ref=source.at[at], dst_ref=target.at[at],
+            send_sem=send_sems.at[which], recv_sem=recv_sems.at[which, group_of(r)],
             device_id=peers[r], device_id_type=pl.DeviceIdType.MESH,
         )
 
-    for copy in stages:
+    for copy in stages[:8]:
         copy.wait()
     for copy in loads:
         copy.start()
@@ -202,8 +217,10 @@
             jnp.ones((SUBLANES, tokens), jnp.float32), rows, (((1,), (1,)), ((), ())),
             precision=lax.Precision.HIGHEST, preferred_element_type=jnp.float32,
         )
-        ends_ref[direction, 6:8, :] = jnp.zeros((2, span), jnp.float32)
-        ends_ref[direction, 6:7, :n_groups] = jnp.exp(-sums[:1])
+        ends_wide[direction, 6:8, :] = jnp.zeros((2, span), jnp.float32)
+        ends_wide[direction, 6:7, : 3 * n_groups] = jnp.concatenate(
+            [piece.astype(jnp.float32) for piece in split3(jnp.exp(-sums))], axis=1
+        )[:1]
 
     def put(direction, part, column, value):
         done = 0
@@ -211,7 +228,7 @@
             at = column + done
             line, start = at // span, at % span
             size = min(value.shape[1] - done, span - start)
-            ends_ref[direction, 3 * part + line : 3 * part + line + 1, start : start + size] = (
+            ends_wide[direction, 3 * part + line : 3 * part + line + 1, start : start + size] = (
                 value[:, done : done + size]
             )
             done += size
@@ -280,21 +297,37 @@
             put(direction, 1, column, e_im)
 
 
+    ends_ref[...] = ends_wide[...].astype(jnp.bfloat16)
     pl.semaphore_wait(barrier, devices - 1)
-    copies = []
     for k in range(1, count):
         copy = pltpu.make_async_remote_copy(
             src_ref=ends_ref.at[(mine + k) // count],
             dst_ref=all_ref.at[mine],
-            send_sem=send_sem.at[k],
-            recv_sem=recv_sem.at[k],
+            send_sem=send_sem,
+            recv_sem=recv_sem,
             device_id={"sp": lax.rem(mine + k, count)},
             device_id_type=pl.DeviceIdType.MESH,
         )
         copy.start()
-        copies.append(copy)
-    all_ref[mine] = jnp.zeros(ends_ref.shape[1:], jnp.float32)
-
+    all_ref[mine] = jnp.zeros(ends_ref.shape[1:], jnp.bfloat16)
+
+    for copy in stages[8:]:
+        copy.wait()
+    out_maps = (wide_out, narrow_out)
+    for pack in packs:
+        which, number, column, width, states = pack
+        cols = slice(column, column + width)
+        at = slice(number * per, (number + 1) * per)
+        lanes = slice(which * half + number * LANES, which * half + (number + 1) * LANES)
+        for direction in range(2):
+            for part in range(2):
+                rows = out_maps[which][direction, part, at].reshape(LANES, states)
+                leave[direction, part, :, cols] = block_diagonal(
+                    -rows if part else rows, channels, states
+                )
+        gates[:, lanes] = block_diagonal(
+            gate_ref[which, at].astype(jnp.float32).reshape(LANES, channels), channels, channels
+        )
     slots = devices * capacity
     slot = lax.broadcasted_iota(jnp.int32, (slots, own_rows), 0)
     expert = (slot // capacity) ^ (mine * n_tp + tp)
@@ -325,13 +358,17 @@
     weights = jnp.concatenate(
         [high, (weight - high.astype(jnp.float32)).astype(jnp.bfloat16)], axis=0
     )
-    for copy in copies:
-        copy.wait()
-
+    sent = all_ref.at[pl.ds(0, count - 1)]
+    ends = pltpu.make_async_remote_copy(
+        src_ref=sent, dst_ref=sent, send_sem=send_sem, recv_sem=recv_sem,
+        device_id={"sp": lax.rem(mine + 1, count)}, device_id_type=pl.DeviceIdType.MESH,
+    )
+    ends.wait()
+
+    all_wide[...] = all_ref[...].astype(jnp.float32)
     shares = jnp.concatenate(
-        [all_ref[b, 6:7, :n_groups] for b in range(count)], axis=0
-    )
-    shares = jnp.concatenate(split3(shares), axis=1)
+        [all_wide[b, 6:7, : 3 * n_groups] for b in range(count)], axis=0
+    ).astype(jnp.bfloat16)
     for pack in packs:
         which, number, column, width, states = pack
         cols = slice(column, column + width)
@@ -346,8 +383,8 @@
             c_im = jnp.zeros((1, width), jnp.float32)
             for b in order(count, direction):
                 use = b < mine if direction == 0 else b > mine
-                e_re = all_ref[b, line : line + 1, start : start + width]
-                e_im = all_ref[b, 3 + line : 4 + line, start : start + width]
+                e_re = all_wide[b, line : line + 1, start : start + width]
+                e_im = all_wide[b, 3 + line : 4 + line, start : start + width]
                 d_re, d_im = kept[b : b + 1] * power_re, kept[b : b + 1] * power_im
                 c_re, c_im = (
                     jnp.where(use, d_re * c_re - d_im * c_im + e_re, c_re),
@@ -362,7 +399,6 @@
                     d_re * c_re - d_im * c_im + sub_ref[direction, 0, j : j + 1, cols],
                     d_re * c_im + d_im * c_re + sub_ref[direction, 1, j : j + 1, cols],
                 )
-    out_maps = (wide_out, narrow_out)
     for pack in packs:
         which, number, column, width, states = pack
         cols = slice(column, column + width)
@@ -383,12 +419,9 @@
                 push[direction, 0, rows, cols] = h_re
                 push[direction, 1, rows, cols] = h_im
             for part in range(2):
-                rows = out_maps[which][direction, part, at].reshape(LANES, states)
-                if part:
-                    rows = -rows
                 term = lax.dot_general(
                     push[direction, part, :, cols].astype(jnp.bfloat16),
-                    block_diagonal(rows, channels, states),
+                    leave[direction, part, :, cols],
                     (((1,), (1,)), ((), ())),
                     preferred_element_type=jnp.float32,
                 )
@@ -397,11 +430,8 @@
             :, lanes
         ].astype(jnp.float32)
         active = jax.nn.gelu(shaped, approximate=True)
-        gate = block_diagonal(
-            gate_ref[which, at].astype(jnp.float32).reshape(LANES, channels), channels, channels
-        )
         opened = jax.nn.sigmoid(
-            jnp.dot(active.astype(jnp.bfloat16), gate, preferred_element_type=jnp.float32)
+            jnp.dot(active.astype(jnp.bfloat16), gates[:, lanes], preferred_element_type=jnp.float32)
         )
         mixed[:, lanes] = jnp.dot(
             unweave, (active * opened).astype(jnp.bfloat16), preferred_element_type=jnp.float32
@@ -434,38 +464,35 @@
     moved = (joined * scale * mixer_gain[...]).astype(jnp.bfloat16)
     loads[0].wait()
 
-    def own_hidden(cols):
-        value = residual[:, cols].astype(jnp.float32) + jnp.dot(
-            moved, out_w[:, cols], preferred_element_type=jnp.float32
-        )
-        own[:, cols] = value.astype(jnp.bfloat16).astype(jnp.float32)
-
-    tiles(model, 512, own_hidden)
-    scale = rms_scale(own[...], model)
-
-    def dispatch(cols):
-        value = (own[:, cols] * scale * ffn_gain[:, cols]).astype(jnp.bfloat16)
+    lead, rest = send_order(devices)
+    for part in range(model // TILE):
+        cols = slice(part * TILE, (part + 1) * TILE)
+        value = (
+            residual[:, cols].astype(jnp.float32)
+            + jnp.dot(moved, out_w[:, cols], preferred_element_type=jnp.float32)
+        ).astype(jnp.bfloat16)
+        own[:, cols] = value.astype(jnp.float32)
         rows = jnp.dot(spot, value, preferred_element_type=jnp.float32)
         send_d[:, :, cols] = rows.reshape(devices, capacity, -1).astype(jnp.bfloat16)
-
-    tiles(model, 512, dispatch)
+        for r in lead:
+            exchange(0, send_d, recv_d, r, part).start()
+    for r in rest:
+        exchange(0, send_d, recv_d, r).start()
     recv_d[0] = send_d[0]
-    outs = [exchange(0, send_d, recv_d, r) for r in send_order(devices)]
-    for copy in outs:
-        copy.start()
     for copy in loads[1:]:
         copy.wait()
-    backs = []
-    for a, b in chunks_of(devices):
-        for r in range(max(a, 1), b):
-            exchange(0, send_d, recv_d, r).wait_recv()
+    for a, b in spans:
+        whole(0, send_d, recv_d, max(a, 1), b).wait_recv()
         rows = (b - a) * capacity
-
-        def arrange(cols, a=a, b=b, rows=rows):
+        squares = jnp.zeros((rows, 1), jnp.float32)
+        for start in range(0, model, TILE):
+            value = recv_d[a:b, :, start : start + TILE].astype(jnp.float32).reshape(rows, -1)
+            squares = squares + jnp.sum(value * value, axis=1, keepdims=True)
+        scale = lax.rsqrt(squares / model + epsilon)
+        for start in range(0, model, TILE):
+            cols = slice(start, start + TILE)
             value = recv_d[a:b, :, cols].astype(jnp.float32).reshape(rows, -1)
-            normed[:rows, cols] = value.astype(jnp.bfloat16)
-
-        tiles(model, 512, arrange)
+            normed[:rows, cols] = (value * scale * ffn_gain[:, cols]).astype(jnp.bfloat16)
 
         def up(cols, rows=rows):
             value = normed[:rows, :]
@@ -483,12 +510,9 @@
         if a == 0:
             recv_o[0] = send_o[0]
         for r in range(max(a, 1), b):
-            copy = exchange(1, send_o, recv_o, r)
-            copy.start()
-            backs.append(copy)
-    for a, b in chunks_of(devices):
-        for r in range(max(a, 1), b):
-            exchange(1, send_o, recv_o, r).wait_recv()
+            exchange(1, send_o, recv_o, r).start()
+    for a, b in spans:
+        whole(1, send_o, recv_o, max(a, 1), b).wait_recv()
         part = weights[:, a * capacity : b * capacity]
 
         def gather(cols, a=a, b=b, part=part):
@@ -499,8 +523,8 @@
 
         tiles(model, 512, gather)
     result[...] = own[...].astype(jnp.bfloat16)
-    for copy in outs + backs:
-        copy.wait_send()
+    whole(0, send_d, recv_d, 1, devices).wait_send()
+    whole(1, send_o, recv_o, 1, devices).wait_send()
 
 
 def local(*args):
@@ -545,10 +569,14 @@
             pltpu.VMEM((tokens, 2 * half), bf16),
             pltpu.VMEM((2, 2, tokens, total), f32),
             pltpu.VMEM((2, tokens, total), f32),
+            pltpu.VMEM((2, 8, span), bf16),
             pltpu.VMEM((2, 8, span), f32),
             pltpu.VMEM((2, 4, SUBLANES, total), f32),
+            pltpu.VMEM((count, 8, span), bf16),
             pltpu.VMEM((count, 8, span), f32),
             pltpu.VMEM((2, 2, SUBLANES, total), f32),
+            pltpu.VMEM((2, 2, LANES, total), bf16),
+            pltpu.VMEM((LANES, 2 * half), bf16),
             pltpu.VMEM((tokens, 2 * half), bf16),
             pltpu.VMEM((n_tp, own_rows, 2 * half), bf16),
             pltpu.VMEM((devices, capacity, width), bf16),
@@ -560,11 +588,11 @@
             pltpu.VMEM((chunk, hidden_width), bf16),
             dma((len(small),)),
             dma((4,)),
-            dma((count,)),
-            dma((count,)),
+            dma,
+            dma,
             dma((2, n_tp)),
-            dma((2, devices)),
-            dma((2, devices)),
+            dma((2,)),
+            dma((2, len(chunks_of(devices)))),
         ],
         compiler_params=pltpu.CompilerParams(
             collective_id=0, has_side_effects=True, vmem_limit_bytes=60 << 20

time: 73.4 us -> 66.6 us (0.907)
  Pallas kernels: 71.5 us -> 64.6 us
    pallas_call x1, Pallas kernels: 71.5 us -> 64.6 us  [local(): pl.pallas_call(layer_kernel, out_shape=jax.ShapeDtypeStruct((own_rows, wi...]
where the time goes in v4:
time: 66.6 us; the launch traced here: 66.2 us
  Pallas kernels  64.6 us (97%)
  local copies, waits for them, and re-layouts  1.67 us (3%)
    pallas_call x1, Pallas kernels, local(): pl.pallas_call(layer_kernel, out_shape=jax.ShapeDtypeStruct((own_rows, wi...  64.6 us
    unnamed x1, local copies, waits for them, and re-layouts  1.67 us

profile of v4, /device:TPU:9, one launch (start us, length us, event | category | flops | bytes accessed | tf_op | source)
XLA Modules:
  0.0 66.2 jit_solution(3734055450750898205)
XLA Ops:
  0.0 64.6 %layer.1 = bf16[64,2048]{1,0:T(8,128)(2,1)} custom-call(bf16[128,256]{1,0:T(8,128)(2,1)} %refs_0_.1, bf16[128,256]{1,0:T(8,128)(2,1)} %refs_1_.1, f32[2,2,16,64]{3,2,1,0:T(8,128)} %refs_2_.1, f32[2,2,16,32]{3,2,1,0:T(8,128)} %refs_3_.1, f32[2,2,16]{2,1,0:T(2,128)} %refs_4_.1, f32[2,2,16,128]{3,2,1,0:T(8,128)} %refs_5_.1, f32[2,2,16,16,64]{4,3,2,1,0:T(8,128)} %refs_6_.1, ...), custom_call_target="tpu_custom_call" | custom-call | tf_op jit(solution)/shard_map/layer/pallas_call | solution.py:561
  64.6 1.7 %copy.23 = bf16[64,2048]{1,0:T(8,128)(2,1)} copy(bf16[64,2048]{1,0:T(8,128)(2,1)} %layer.1) | data formatting | bytes 524288

commit v5 on v4

--- a/solution.py
+++ b/solution.py
@@ -9,6 +9,7 @@
 SUBLANES = 8
 LANES = 128
 TILE = 512
+EARLY_PARTS = 2
 
 
 def complex_power(re, im, exponent):
@@ -111,7 +112,17 @@
     half, quarter = devices // 2, devices // 4
     first = list(range(half, half + quarter))
     near = list(range(1, half))
-    return first, near + list(range(half + quarter, devices))
+    last = list(range(half + quarter, devices))
+    rest = []
+    for i, r in enumerate(last):
+        rest.append(r)
+        rest += near[i * len(near) // len(last) : (i + 1) * len(near) // len(last)]
+    return first, rest
+
+
+def early_span(devices):
+    first = devices // 2 + devices // 4
+    return first, first + max(1, devices * EARLY_PARTS // 32)
 
 
 N_SMALL = 17
@@ -131,8 +142,8 @@
     gate_w, up_w, down_w, out_w = big
     (
         signal, push, keep, ends_ref, ends_wide, sub_ref, all_ref, all_wide, carry, leave, gates, mixed, out_ref, send_d, recv_d,
-        send_o, recv_o, own, normed, inner,
-        small_sem, big_sem, send_sem, recv_sem, swap_sem, send_sems, recv_sems,
+        send_r, recv_r, send_m, recv_m, send_o, recv_o, own, normed, inner,
+        small_sem, big_sem, send_sem, recv_sem, swap_sem, send_sems, recv_sems, tail_sems, early_sems,
     ) = refs
     tokens, half = wide_u.shape
     groups, channels = wide_in.shape[2:4]
@@ -181,7 +192,10 @@
         at = (r,) if part is None else (r, slice(None), slice(part * TILE, (part + 1) * TILE))
         return pltpu.make_async_remote_copy(
             src_ref=source.at[at], dst_ref=target.at[at],
-            send_sem=send_sems.at[which], recv_sem=recv_sems.at[which, group_of(r)],
+            send_sem=send_sems.at[which],
+            recv_sem=tail_sems.at[part]
+            if which and part is not None
+            else recv_sems.at[which, group_of(r)],
             device_id=peers[r], device_id_type=pl.DeviceIdType.MESH,
         )
 
@@ -354,6 +368,30 @@
             jnp.logical_and(each, here), share[k : k + 1] / total_share, 0.0
         )
     weight = weight.T
+    early_a, early_b = early_span(devices)
+    early_spot = spot[early_a * capacity : early_b * capacity]
+
+    def early_copy(which, source, target, r):
+        return pltpu.make_async_remote_copy(
+            src_ref=source.at[r - early_a], dst_ref=target.at[r - early_a],
+            send_sem=early_sems.at[0, which], recv_sem=early_sems.at[1, which],
+            device_id=peers[r], device_id_type=pl.DeviceIdType.MESH,
+        )
+
+    def early_all(which, source, target):
+        return pltpu.make_async_remote_copy(
+            src_ref=source, dst_ref=target,
+            send_sem=early_sems.at[0, which], recv_sem=early_sems.at[1, which],
+            device_id=peers[1], device_id_type=pl.DeviceIdType.MESH,
+        )
+
+    for start in range(0, model, TILE):
+        rows = jnp.dot(
+            early_spot, residual[:, start : start + TILE], preferred_element_type=jnp.float32
+        )
+        send_r[:, :, start : start + TILE] = rows.reshape(
+            early_b - early_a, capacity, -1
+        ).astype(jnp.bfloat16)
     high = weight.astype(jnp.bfloat16)
     weights = jnp.concatenate(
         [high, (weight - high.astype(jnp.float32)).astype(jnp.bfloat16)], axis=0
@@ -364,6 +402,8 @@
         device_id={"sp": lax.rem(mine + 1, count)}, device_id_type=pl.DeviceIdType.MESH,
     )
     ends.wait()
+    for r in range(early_a, early_b):
+        early_copy(0, send_r, recv_r, r).start()
 
     all_wide[...] = all_ref[...].astype(jnp.float32)
     shares = jnp.concatenate(
@@ -462,6 +502,10 @@
     joined = jnp.concatenate([value.astype(jnp.float32) for value, _, _ in parts], axis=1)
     scale = rms_scale(joined, joined.shape[1])
     moved = (joined * scale * mixer_gain[...]).astype(jnp.bfloat16)
+    rows = jnp.dot(early_spot, moved, preferred_element_type=jnp.float32)
+    send_m[...] = rows.reshape(early_b - early_a, capacity, -1).astype(jnp.bfloat16)
+    for r in range(early_a, early_b):
+        early_copy(1, send_m, recv_m, r).start()
     loads[0].wait()
 
     lead, rest = send_order(devices)
@@ -476,13 +520,33 @@
         send_d[:, :, cols] = rows.reshape(devices, capacity, -1).astype(jnp.bfloat16)
         for r in lead:
             exchange(0, send_d, recv_d, r, part).start()
-    for r in rest:
+    for r in [x for x in rest if not early_a <= x < early_b]:
         exchange(0, send_d, recv_d, r).start()
     recv_d[0] = send_d[0]
     for copy in loads[1:]:
         copy.wait()
-    for a, b in spans:
-        whole(0, send_d, recv_d, max(a, 1), b).wait_recv()
+    fronts = [x for x in spans if x[0] in lead]
+    near = [x for x in spans if x[0] < devices // 2]
+    others_last = [x for x in spans if x not in fronts and x not in near]
+    for a, b in fronts + near + others_last:
+        if (a, b) in others_last and a <= early_a < b:
+            for which, source, target in ((0, send_r, recv_r), (1, send_m, recv_m)):
+                early_all(which, source, target).wait_recv()
+            count_e = (early_b - early_a) * capacity
+            arrived = recv_m[...].astype(jnp.float32).reshape(count_e, -1).astype(jnp.bfloat16)
+            for start in range(0, model, TILE):
+                cols = slice(start, start + TILE)
+                value = recv_r[:, :, cols].astype(jnp.float32).reshape(count_e, -1) + jnp.dot(
+                    arrived, out_w[:, cols], preferred_element_type=jnp.float32
+                )
+                recv_d[early_a:early_b, :, cols] = value.reshape(
+                    early_b - early_a, capacity, -1
+                ).astype(jnp.bfloat16)
+        first = max(a, 1)
+        if early_a <= first < early_b:
+            first = early_b
+        if first < b:
+            whole(0, send_d, recv_d, first, b).wait_recv()
         rows = (b - a) * capacity
         squares = jnp.zeros((rows, 1), jnp.float32)
         for start in range(0, model, TILE):
@@ -506,13 +570,20 @@
             value = jnp.dot(inner[:rows, :], down_w[:, cols], preferred_element_type=jnp.float32)
             send_o[a:b, :, cols] = value.reshape(b - a, capacity, -1).astype(jnp.bfloat16)
 
-        tiles(model, 512, down)
+        if (a, b) == spans[-1]:
+            for part in range(model // TILE):
+                down(slice(part * TILE, (part + 1) * TILE))
+                for r in range(a, b):
+                    exchange(1, send_o, recv_o, r, part).start()
+        else:
+            tiles(model, 512, down)
+            for r in range(max(a, 1), b):
+                exchange(1, send_o, recv_o, r).start()
         if a == 0:
             recv_o[0] = send_o[0]
-        for r in range(max(a, 1), b):
-            exchange(1, send_o, recv_o, r).start()
     for a, b in spans:
-        whole(1, send_o, recv_o, max(a, 1), b).wait_recv()
+        if (a, b) != spans[-1]:
+            whole(1, send_o, recv_o, max(a, 1), b).wait_recv()
         part = weights[:, a * capacity : b * capacity]
 
         def gather(cols, a=a, b=b, part=part):
@@ -521,9 +592,23 @@
             both = jnp.dot(part, rows, preferred_element_type=jnp.float32)
             own[:, cols] = own[:, cols] + (both[:own_rows] + both[own_rows:])
 
-        tiles(model, 512, gather)
+        if (a, b) != spans[-1]:
+            tiles(model, 512, gather)
+            continue
+        for line in range(model // TILE):
+            cols = slice(line * TILE, (line + 1) * TILE)
+            at = recv_o.at[pl.ds(a, b - a), :, cols]
+            pltpu.make_async_remote_copy(
+                src_ref=at, dst_ref=at, send_sem=send_sems.at[1], recv_sem=tail_sems.at[line],
+                device_id=peers[1], device_id_type=pl.DeviceIdType.MESH,
+            ).wait_recv()
+            gather(cols)
     result[...] = own[...].astype(jnp.bfloat16)
-    whole(0, send_d, recv_d, 1, devices).wait_send()
+    whole(0, send_d, recv_d, 1, early_a).wait_send()
+    if early_b < devices:
+        whole(0, send_d, recv_d, early_b, devices).wait_send()
+    early_all(0, send_r, recv_r).wait_send()
+    early_all(1, send_m, recv_m).wait_send()
     whole(1, send_o, recv_o, 1, devices).wait_send()
 
 
@@ -553,6 +638,7 @@
     hidden_width = by["gate_proj"].shape[2]
     capacity = max(4 * tokens // (n_tp * devices), SUBLANES)
     span = total // 3
+    early_rows = early_span(devices)[1] - early_span(devices)[0]
     chunk = max(b - a for a, b in chunks_of(devices)) * capacity
     vmem = pl.BlockSpec(memory_space=pltpu.VMEM)
     hbm = pl.BlockSpec(memory_space=pltpu.HBM)
@@ -581,6 +667,10 @@
             pltpu.VMEM((n_tp, own_rows, 2 * half), bf16),
             pltpu.VMEM((devices, capacity, width), bf16),
             pltpu.VMEM((devices, capacity, width), bf16),
+            pltpu.VMEM((early_rows, capacity, width), bf16),
+            pltpu.VMEM((early_rows, capacity, width), bf16),
+            pltpu.VMEM((early_rows, capacity, 2 * half * n_tp), bf16),
+            pltpu.VMEM((early_rows, capacity, 2 * half * n_tp), bf16),
             pltpu.VMEM((devices, capacity, width), bf16),
             pltpu.VMEM((devices, capacity, width), bf16),
             pltpu.VMEM((own_rows, width), f32),
@@ -593,6 +683,8 @@
             dma((2, n_tp)),
             dma((2,)),
             dma((2, len(chunks_of(devices)))),
+            dma((width // TILE,)),
+            dma((2, 2)),
         ],
         compiler_params=pltpu.CompilerParams(
             collective_id=0, has_side_effects=True, vmem_limit_bytes=60 << 20

time: 66.6 us -> 64.6 us (0.970)
  Pallas kernels: 64.6 us -> 62 us
    pallas_call x1, Pallas kernels: 64.6 us -> 62 us  [local(): pl.pallas_call(layer_kernel, out_shape=jax.ShapeDtypeStruct((own_rows, wi...]
where the time goes in v5:
time: 64.6 us; the launch traced here: 63.7 us
  Pallas kernels  62 us (96%)
  local copies, waits for them, and re-layouts  1.67 us (3%)
    pallas_call x1, Pallas kernels, local(): pl.pallas_call(layer_kernel, out_shape=jax.ShapeDtypeStruct((own_rows, wi...  62 us
    unnamed x1, local copies, waits for them, and re-layouts  1.67 us

profile of v5, /device:TPU:9, one launch (start us, length us, event | category | flops | bytes accessed | tf_op | source)
XLA Modules:
  0.0 63.7 jit_solution(2942206921632375788)
XLA Ops:
  0.0 62.0 %layer.1 = bf16[64,2048]{1,0:T(8,128)(2,1)} custom-call(bf16[128,256]{1,0:T(8,128)(2,1)} %refs_0_.1, bf16[128,256]{1,0:T(8,128)(2,1)} %refs_1_.1, f32[2,2,16,64]{3,2,1,0:T(8,128)} %refs_2_.1, f32[2,2,16,32]{3,2,1,0:T(8,128)} %refs_3_.1, f32[2,2,16]{2,1,0:T(2,128)} %refs_4_.1, f32[2,2,16,128]{3,2,1,0:T(8,128)} %refs_5_.1, f32[2,2,16,16,64]{4,3,2,1,0:T(8,128)} %refs_6_.1, ...), custom_call_target="tpu_custom_call" | custom-call | tf_op jit(solution)/shard_map/layer/pallas_call | solution.py:647
  62.0 1.7 %copy.23 = bf16[64,2048]{1,0:T(8,128)(2,1)} copy(bf16[64,2048]{1,0:T(8,128)(2,1)} %layer.1) | data formatting | bytes 524288

commit v6 on v5

--- a/solution.py
+++ b/solution.py
@@ -199,10 +199,8 @@
             device_id=peers[r], device_id_type=pl.DeviceIdType.MESH,
         )
 
-    for copy in stages[:8]:
+    for copy in stages[:3]:
         copy.wait()
-    for copy in loads:
-        copy.start()
 
     row = lax.broadcasted_iota(jnp.int32, (tokens, tokens), 0)
     column = lax.broadcasted_iota(jnp.int32, (tokens, tokens), 1)
@@ -247,6 +245,10 @@
             )
             done += size
 
+    for copy in stages[3:8]:
+        copy.wait()
+    for copy in loads:
+        copy.start()
     eye_row = lax.broadcasted_iota(jnp.int32, (per, groups), 0)
     eye_column = lax.broadcasted_iota(jnp.int32, (per, groups), 1)
     poles, in_maps = (wide_poles, narrow_poles), (wide_in, narrow_in)
@@ -327,6 +329,7 @@
 
     for copy in stages[8:]:
         copy.wait()
+    powers = {at: complex_power(*rate, tokens) for at, rate in rates.items()}
     out_maps = (wide_out, narrow_out)
     for pack in packs:
         which, number, column, width, states = pack
@@ -418,7 +421,7 @@
         )
         for direction in range(2):
             rate_re, rate_im = rates[direction, column]
-            power_re, power_im = complex_power(rate_re, rate_im, tokens)
+            power_re, power_im = powers[direction, column]
             c_re = jnp.zeros((1, width), jnp.float32)
             c_im = jnp.zeros((1, width), jnp.float32)
             for b in order(count, direction):

time: 64.6 us -> 64.5 us (level)
  no operation moved by 1% of the time
where the time goes in v6:
time: 64.5 us; the launch traced here: 63.6 us
  Pallas kernels  61.9 us (96%)
  local copies, waits for them, and re-layouts  1.67 us (3%)
    pallas_call x1, Pallas kernels, local(): pl.pallas_call(layer_kernel, out_shape=jax.ShapeDtypeStruct((own_rows, wi...  61.9 us
    unnamed x1, local copies, waits for them, and re-layouts  1.67 us

profile of v6, /device:TPU:9, one launch (start us, length us, event | category | flops | bytes accessed | tf_op | source)
XLA Modules:
  0.0 63.6 jit_solution(10086763957486746715)
XLA Ops:
  0.0 61.9 %layer.1 = bf16[64,2048]{1,0:T(8,128)(2,1)} custom-call(bf16[128,256]{1,0:T(8,128)(2,1)} %refs_0_.1, bf16[128,256]{1,0:T(8,128)(2,1)} %refs_1_.1, f32[2,2,16,64]{3,2,1,0:T(8,128)} %refs_2_.1, f32[2,2,16,32]{3,2,1,0:T(8,128)} %refs_3_.1, f32[2,2,16]{2,1,0:T(2,128)} %refs_4_.1, f32[2,2,16,128]{3,2,1,0:T(8,128)} %refs_5_.1, f32[2,2,16,16,64]{4,3,2,1,0:T(8,128)} %refs_6_.1, ...), custom_call_target="tpu_custom_call" | custom-call | tf_op jit(solution)/shard_map/layer/pallas_call | solution.py:650
  62.0 1.7 %copy.23 = bf16[64,2048]{1,0:T(8,128)(2,1)} copy(bf16[64,2048]{1,0:T(8,128)(2,1)} %layer.1) | data formatting | bytes 524288
